TPU v7x, 32 devices: a whole 2x2x4 slice. The times are simulated.
32 devices in a mesh: sp: 8 (over z, y), dp: 4 (over x, core).
Axes of the slice: x: 2, y: 2, z: 4, core: 2. Of those that a mesh axis runs over, the one named last changes fastest.
Arguments:
- tokens: bfloat16 [4, 2048, 2048], P('dp', 'sp'), may hold values from -6 to 6
- in_gain: float32 [2048], replicated, may hold values from 0.1 to 1.9
- w_query_down: bfloat16 [2048, 512], P('dp'), may hold values from -0.125 to 0.125
- w_latent_down: bfloat16 [2048, 256], P('dp'), may hold values from -0.125 to 0.125
- w_rope_key: bfloat16 [2048, 64], replicated, may hold values from -0.125 to 0.125
- query_latent_gain: float32 [512], replicated, may hold values from 0.1 to 1.9
- latent_gain: float32 [256], replicated, may hold values from 0.1 to 1.9
- w_query_up: bfloat16 [512, 3072], P('dp', 'sp'), may hold values from -0.25 to 0.25
- w_key_up: bfloat16 [256, 2048], P('dp', 'sp'), may hold values from -0.375 to 0.375
- w_value_up: bfloat16 [256, 2048], P('dp', 'sp'), may hold values from -0.375 to 0.375
- query_gain: float32 [192], replicated, may hold values from 0.5 to 14
- key_gain: float32 [192], replicated, may hold values from 0.5 to 14
- out_gain: float32 [2048], replicated, may hold values from 0.1 to 1.9
- w_out: bfloat16 [2048, 2048], P(('sp', 'dp')), may hold values from -0.125 to 0.125
Outputs:
- result: bfloat16 [4, 2048, 2048], P('dp', 'sp')
All inputs are finite; a program needn't handle non-finite values.
Results may differ from a plain program's by a relative error of at most 0.034.
The roundings to bfloat16 on the way count: a program that leaves them out, or rounds other values in their place, can miss the bound.
Values may be sent and summed in bfloat16 or wider, within the bound.
A program may use at most 64 MiB of HBM per device.

v0:
```python
import jax
import jax.numpy as jnp
from jax import lax
from jax.sharding import PartitionSpec as P

HEADS = 16


EPS = 1e-06
THETA = 10000.0
NEG_BIG = -1e30


def rms_scale(values, scaling):
    return values * lax.rsqrt(jnp.mean(values * values, axis=-1, keepdims=True) + EPS) * scaling


def rotate(tail_part, positions):
    half_width = tail_part.shape[-1] // 2
    frequency = THETA ** (-jnp.arange(half_width, dtype=jnp.float32) / half_width)
    angles = positions[:, None] * frequency[None, :]
    cosine = jnp.cos(angles)[:, None, :]
    sine = jnp.sin(angles)[:, None, :]
    first_half = tail_part[..., :half_width]
    second_half = tail_part[..., half_width:]
    return jnp.concatenate(
        [first_half * cosine - second_half * sine, second_half * cosine + first_half * sine],
        axis=-1,
    )


def finish_heads(joined, positions, scaling, rope_width):
    row_count = joined.shape[0]
    normal = rms_scale(joined, scaling)
    turned = rotate(normal[..., -rope_width:], positions)
    return (
        jnp.concatenate([normal[..., :-rope_width], turned], axis=-1)
        .astype(jnp.bfloat16)
        .reshape(row_count, -1)
    )


def make_queries(query_total, positions, scaling, head_count, rope_width):
    row_count = query_total.shape[0]
    return finish_heads(
        query_total.reshape(row_count, head_count, -1), positions, scaling, rope_width
    )


def make_keys(key_total, rope_key, positions, scaling, head_count):
    row_count = key_total.shape[0]
    rope_width = rope_key.shape[1]
    shaped = key_total.reshape(row_count, head_count, -1)
    shared = jnp.broadcast_to(
        rope_key.astype(jnp.float32)[:, None, :], (row_count, head_count, rope_width)
    )
    return finish_heads(jnp.concatenate([shaped, shared], axis=-1), positions, scaling, rope_width)


def single_fold(inputs, piece):
    return jnp.dot(inputs, piece, preferred_element_type=jnp.float32)


def double_fold(inputs, pieces):
    return (
        jnp.dot(inputs, pieces[0], preferred_element_type=jnp.float32),
        jnp.dot(inputs, pieces[1], preferred_element_type=jnp.float32),
    )


def attend(queries, keys, values, head_count):
    length = queries.shape[0]
    block_rows = min(512, length)
    query_blocks = queries.reshape(length // block_rows, block_rows, head_count, -1)
    key_heads = keys.reshape(length, head_count, -1)
    value_heads = values.reshape(length, head_count, -1)
    score_scale = key_heads.shape[-1] ** (-0.5)
    key_pos = jnp.arange(length)

    def one_block(block_args):
        query_block, block_index = block_args
        scores = (
            jnp.einsum("qhd,khd->hqk", query_block, key_heads, preferred_element_type=jnp.float32)
            * score_scale
        )
        query_pos = block_index * block_rows + jnp.arange(block_rows)
        allowed = key_pos[None, :] <= query_pos[:, None]
        scores = jnp.where(allowed[None], scores, NEG_BIG)
        weights = jax.nn.softmax(scores, axis=-1).astype(jnp.bfloat16)
        return jnp.einsum(
            "hqk,khd->qhd", weights, value_heads, preferred_element_type=jnp.float32
        ).astype(jnp.bfloat16)

    outcome = lax.map(one_block, (query_blocks, jnp.arange(length // block_rows)))
    return outcome.reshape(length, -1)


def per_device(
    tokens,
    in_gain,
    w_query_down,
    w_latent_down,
    w_rope_key,
    query_latent_gain,
    latent_gain,
    w_query_up,
    w_key_up,
    w_value_up,
    query_gain,
    key_gain,
    out_gain,
    w_out,
):
    seq_devices = lax.axis_size("sp")
    head_count = HEADS // seq_devices
    own_rows = tokens.shape[1]
    length = own_rows * seq_devices
    rope_width = w_rope_key.shape[1]
    local_rows = tokens.reshape(own_rows, tokens.shape[2])
    normed = rms_scale(local_rows.astype(jnp.float32), in_gain).astype(jnp.bfloat16)
    query_sum, latent_sum = double_fold(
        normed,
        (
            lax.all_gather(w_query_down, "dp", axis=0, tiled=True),
            lax.all_gather(w_latent_down, "dp", axis=0, tiled=True),
        ),
    )
    latent_q = rms_scale(query_sum, query_latent_gain).astype(jnp.bfloat16)
    latent_kv = rms_scale(latent_sum, latent_gain).astype(jnp.bfloat16)
    rope_key = jnp.dot(normed, w_rope_key, preferred_element_type=jnp.float32).astype(jnp.bfloat16)
    every_q, every_kv, every_rope = (
        lax.all_gather(latent_q, "sp", axis=0, tiled=True),
        lax.all_gather(latent_kv, "sp", axis=0, tiled=True),
        lax.all_gather(rope_key, "sp", axis=0, tiled=True),
    )
    positions = jnp.arange(length, dtype=jnp.float32)
    query_total = single_fold(every_q, lax.all_gather(w_query_up, "dp", axis=0, tiled=True))
    key_total, value_total = double_fold(
        every_kv,
        (
            lax.all_gather(w_key_up, "dp", axis=0, tiled=True),
            lax.all_gather(w_value_up, "dp", axis=0, tiled=True),
        ),
    )
    queries = make_queries(query_total, positions, query_gain, head_count, rope_width)
    keys = make_keys(key_total, every_rope, positions, key_gain, head_count)
    values = value_total.astype(jnp.bfloat16)
    attended = attend(queries, keys, values, head_count)
    token_heads = lax.all_to_all(attended, "sp", split_axis=0, concat_axis=1, tiled=True)
    mixed = rms_scale(token_heads.astype(jnp.float32), out_gain).astype(jnp.bfloat16)
    projected = single_fold(mixed, lax.all_gather(w_out, ("sp", "dp"), axis=0, tiled=True))
    return projected.astype(jnp.bfloat16).reshape(1, own_rows, w_out.shape[1])


def solution(mesh):
    in_specs = (
        P("dp", "sp", None),
        P(),
        P("dp", None),
        P("dp", None),
        P(),
        P(),
        P(),
        P("dp", "sp"),
        P("dp", "sp"),
        P("dp", "sp"),
        P(),
        P(),
        P(),
        P(("sp", "dp"), None),
    )
    out_specs = P("dp", "sp", None)
    return jax.shard_map(
        per_device, mesh=mesh, in_specs=in_specs, out_specs=out_specs, check_vma=False
    )
```

profile of v0, /device:TPU:0, one launch (start us, length us, event | category | flops | bytes accessed | tf_op | source)
XLA Modules:
  0.0 265.2 jit_solution(6312422540849685610)
XLA Ops:
  8.1 1.6 fusion.31
  9.7 18.7 %all-gather.10.cloned.1.call-done = bf16[2048,256]{1,0:T(8,128)(2,1)} async-done(((bf16[512,256]{1,0:T(8,128)(2,1)}), bf16[2048,256]{1,0:T(8,128)(2,1)}) %all-gather.10.cloned.1.call-update) | async-done | bytes 1048592 | tf_op jit(solution)/shard_map/all_gather | solution.py:125
  28.4 2.2 multiply_reduce_fusion.3
  31.4 21.1 %all-gather.6.cloned.1.call-done = bf16[2048,512]{1,0:T(8,128)(2,1)} async-done(((bf16[512,512]{1,0:T(8,128)(2,1)}), bf16[2048,512]{1,0:T(8,128)(2,1)}) %all-gather.6.cloned.1.call-update) | async-done | bytes 2097168 | tf_op jit(solution)/shard_map/all_gather | solution.py:124
  52.5 2.4 multiply_reduce_fusion.2
  56.5 5.4 %all_gather.32 = bf16[256,256]{1,0:T(8,128)(2,1)S(1)} all-gather(bf16[64,256]{1,0:T(8,128)(2,1)S(1)} %copy-done.7), channel_id=1, replica_groups=mesh['sp'=8,'dp'=4] {'dp'}, dimensions={0}, use_global_device_ids=true | all-gather | bytes 163840 | tf_op jit(solution)/shard_map/all_gather | solution.py:141
  62.4 31.3 %all_gather.33 = bf16[2048,64]{0,1:T(8,128)(2,1)S(1)} all-gather(bf16[256,64]{0,1:T(8,128)(2,1)S(1)} %convolution_convert_fusion.2), channel_id=1, replica_groups=mesh['sp'=8,'dp'=4] {'sp'}, dimensions={0}, use_global_device_ids=true | all-gather | bytes 294912 | tf_op jit(solution)/shard_map/all_gather | solution.py:134
  93.7 6.6 %all_gather.29 = bf16[512,384]{1,0:T(8,128)(2,1)} all-gather(bf16[128,384]{1,0:T(8,128)(2,1)S(1)} %copy-done.6), channel_id=1, replica_groups=mesh['sp'=8,'dp'=4] {'dp'}, dimensions={0}, use_global_device_ids=true | all-gather | bytes 491520 | tf_op jit(solution)/shard_map/all_gather | solution.py:137
  100.3 1.8 fusion.37
  102.1 5.6 %all_gather.34 = bf16[256,256]{1,0:T(8,128)(2,1)S(1)} all-gather(bf16[64,256]{1,0:T(8,128)(2,1)S(1)} %copy-done.8), channel_id=1, replica_groups=mesh['sp'=8,'dp'=4] {'dp'}, dimensions={0}, use_global_device_ids=true | all-gather | bytes 163840 | tf_op jit(solution)/shard_map/all_gather | solution.py:142
  107.7 1.7 fusion.49
  110.7 1.2 slice.48
  112.3 1.5 convolution_convert_fusion
  113.8 2.3 copy.22
  116.0 29.2 %all-gather.8.cloned.1.call-done = bf16[2048,512]{1,0:T(8,128)(2,1)} async-done(((bf16[256,512]{1,0:T(8,128)(2,1)}), bf16[2048,512]{1,0:T(8,128)(2,1)}) %all-gather.8.cloned.1.call-update) | async-done | bytes 2097168 | tf_op jit(solution)/shard_map/all_gather | solution.py:132
  145.2 2.7 %fusion.48 = f32[2048,384]{0,1:T(8,128)S(1)} fusion(bf16[2048,512]{1,0:T(8,128)(2,1)} %all-gather.8.cloned.1.call-done, bf16[512,384]{1,0:T(8,128)(2,1)} %all_gather.29), kind=kOutput, calls=%fused_computation.73 | convolution fusion | flops 805306368 | bytes 5636096 | tf_op jit(solution)/shard_map/dot_general | solution.py:61
  150.7 1.0 copy-done.2
  151.7 1.3 pad_maximum_fusion.2
  153.0 64.4 %while.11 = (s32[]{:T(128)}, bf16[4,512,2,128]{3,2,1,0:T(2,128)(2,1)}, s32[4]{0:T(128)S(1)}, bf16[4,512,2,192]{1,3,2,0:T(8,128)(2,1)S(1)}, bf16[2048,2,192]{0,2,...) while((s32[]{:T(128)}, bf16[4,512,2,128]{3,2,1,0:T(2,128)(2,1)}, ...), condition=%wide.region_8.9_spmd.clone, body=%wide.region_5.8_spmd.clone.sunk | while | flops 1355942400 | bytes 22688372 | solution.py:94
  154.9 8.1 %fusion.72 = (f32[2,512]{1,0:T(2,128)S(1)}, f32[2,512,2048]{2,1,0:T(8,128)}) fusion(pred[512,2048]{1,0:T(8,128)(4,1)S(1)} %iota_compare_fusion.2, bf16[2048,2,192]{0,2,1:T(8,128)(2,1)} %get-tuple-element.158, bf16[4,512,2,192]{1,3,2,0:T(8,128)(2,1)S(1)} %get-tuple-element.157, s32[]{:T(128)} %get-tuple-element.146), kind=kOutput, calls=%fused_computation.72.clone.1 | convolution fusion | flops 813697024 | bytes 11407364 | tf_op jit(solution)/shard_map/while/body/eval_jaxpr/sub | solution.py:89
  163.0 4.9 %fusion.73 = bf16[1,512,2,128]{3,1,2,0:T(8,128)(2,1)S(1)} fusion(bf16[2048,2,128]{2,0,1:T(8,128)(2,1)} %get-tuple-element.159, f32[2,512,2048]{2,1,0:T(8,128)} %get-tuple-element.136, f32[2,512]{1,0:T(2,128)S(1)} %get-tuple-element.137), kind=kOutput, calls=%fused_computation.12.clone.1 | convolution fusion | flops 541196288 | bytes 9703424 | tf_op jit(solution)/shard_map/while/body/eval_jaxpr/hqk,khd->qhd/dot_general | solution.py:90
  170.9 8.0 %fusion.72 = (f32[2,512]{1,0:T(2,128)S(1)}, f32[2,512,2048]{2,1,0:T(8,128)}) fusion(pred[512,2048]{1,0:T(8,128)(4,1)S(1)} %iota_compare_fusion.2, bf16[2048,2,192]{0,2,1:T(8,128)(2,1)} %get-tuple-element.158, bf16[4,512,2,192]{1,3,2,0:T(8,128)(2,1)S(1)} %get-tuple-element.157, s32[]{:T(128)} %get-tuple-element.146), kind=kOutput, calls=%fused_computation.72.clone.1 | convolution fusion | flops 813697024 | bytes 11407364 | tf_op jit(solution)/shard_map/while/body/eval_jaxpr/sub | solution.py:89
  178.9 4.9 %fusion.73 = bf16[1,512,2,128]{3,1,2,0:T(8,128)(2,1)S(1)} fusion(bf16[2048,2,128]{2,0,1:T(8,128)(2,1)} %get-tuple-element.159, f32[2,512,2048]{2,1,0:T(8,128)} %get-tuple-element.136, f32[2,512]{1,0:T(2,128)S(1)} %get-tuple-element.137), kind=kOutput, calls=%fused_computation.12.clone.1 | convolution fusion | flops 541196288 | bytes 9703424 | tf_op jit(solution)/shard_map/while/body/eval_jaxpr/hqk,khd->qhd/dot_general | solution.py:90
  186.8 8.7 %fusion.72 = (f32[2,512]{1,0:T(2,128)S(1)}, f32[2,512,2048]{2,1,0:T(8,128)}) fusion(pred[512,2048]{1,0:T(8,128)(4,1)S(1)} %iota_compare_fusion.2, bf16[2048,2,192]{0,2,1:T(8,128)(2,1)} %get-tuple-element.158, bf16[4,512,2,192]{1,3,2,0:T(8,128)(2,1)S(1)} %get-tuple-element.157, s32[]{:T(128)} %get-tuple-element.146), kind=kOutput, calls=%fused_computation.72.clone.1 | convolution fusion | flops 813697024 | bytes 11407364 | tf_op jit(solution)/shard_map/while/body/eval_jaxpr/sub | solution.py:89
  195.5 4.9 %fusion.73 = bf16[1,512,2,128]{3,1,2,0:T(8,128)(2,1)S(1)} fusion(bf16[2048,2,128]{2,0,1:T(8,128)(2,1)} %get-tuple-element.159, f32[2,512,2048]{2,1,0:T(8,128)} %get-tuple-element.136, f32[2,512]{1,0:T(2,128)S(1)} %get-tuple-element.137), kind=kOutput, calls=%fused_computation.12.clone.1 | convolution fusion | flops 541196288 | bytes 9703424 | tf_op jit(solution)/shard_map/while/body/eval_jaxpr/hqk,khd->qhd/dot_general | solution.py:90
  203.3 8.0 %fusion.72 = (f32[2,512]{1,0:T(2,128)S(1)}, f32[2,512,2048]{2,1,0:T(8,128)}) fusion(pred[512,2048]{1,0:T(8,128)(4,1)S(1)} %iota_compare_fusion.2, bf16[2048,2,192]{0,2,1:T(8,128)(2,1)} %get-tuple-element.158, bf16[4,512,2,192]{1,3,2,0:T(8,128)(2,1)S(1)} %get-tuple-element.157, s32[]{:T(128)} %get-tuple-element.146), kind=kOutput, calls=%fused_computation.72.clone.1 | convolution fusion | flops 813697024 | bytes 11407364 | tf_op jit(solution)/shard_map/while/body/eval_jaxpr/sub | solution.py:89
  211.3 5.1 %fusion.73 = bf16[1,512,2,128]{3,1,2,0:T(8,128)(2,1)S(1)} fusion(bf16[2048,2,128]{2,0,1:T(8,128)(2,1)} %get-tuple-element.159, f32[2,512,2048]{2,1,0:T(8,128)} %get-tuple-element.136, f32[2,512]{1,0:T(2,128)S(1)} %get-tuple-element.137), kind=kOutput, calls=%fused_computation.12.clone.1 | convolution fusion | flops 541196288 | bytes 9703424 | tf_op jit(solution)/shard_map/while/body/eval_jaxpr/hqk,khd->qhd/dot_general | solution.py:90
  217.4 1.7 all_to_all.10
  219.2 28.6 %all_to_all.13 = bf16[8,256,256]{2,1,0:T(8,128)(2,1)S(1)} all-to-all(bf16[8,256,256]{2,1,0:T(8,128)(2,1)S(1)} %all_to_all.10), channel_id=1, replica_groups=mesh['sp'=8,'dp'=4] {'sp'}, dimensions={0} | all-to-all | bytes 2097152 | tf_op jit(solution)/shard_map/all_to_all | solution.py:149
  247.8 1.6 convert_bitcast_fusion
  249.3 1.9 copy.24
  251.9 6.7 %fusion.29 = bf16[1,256,2048]{2,1,0:T(8,128)(2,1)} fusion(bf16[256,2048]{0,1:T(8,128)(2,1)S(1)} %fusion.35, bf16[2048,2048]{1,0:T(8,128)(2,1)} %all-gather.14.cloned.1.call-done), kind=kOutput, calls=%fused_computation.36 | convolution fusion | flops 2148007936 | bytes 10485760 | tf_op jit(solution)/shard_map/dot_general | solution.py:61
  (81 shorter events, 18.5 us)
Async XLA Ops:
  6.5 55.4 %copy-start = (bf16[2048,64]{0,1:T(8,128)(2,1)S(1)}, bf16[2048,64]{0,1:T(8,128)(2,1)}, u32[]{:S(2)}) copy-start(bf16[2048,64]{0,1:T(8,128)(2,1)} %param.20) | copy-start | bytes 786436
  6.5 21.8 %all-gather.10.cloned.1.call-start = ((), (), s32[]{:S(2)}) async-start(), calls=%async_computation.3 | async-start | bytes 1310720 | tf_op jit(solution)/shard_map/all_gather | solution.py:125
  7.3 45.3 %all-gather.6.cloned.1.call-start = ((), (), s32[]{:S(2)}) async-start(), calls=%async_computation.1 | async-start | bytes 2621440 | tf_op jit(solution)/shard_map/all_gather | solution.py:124
  8.0 22.6 %copy-start.11 = (f32[256]{0:T(256)S(1)}, f32[256]{0:T(256)}, u32[]{:S(2)}) copy-start(f32[256]{0:T(256)} %param.22) | copy-start | bytes 3076
  8.0 44.5 %copy-start.5 = (bf16[1,256,2048]{2,1,0:T(8,128)(2,1)S(1)}, bf16[1,256,2048]{2,1,0:T(8,128)(2,1)}, u32[]{:S(2)}) copy-start(bf16[1,256,2048]{2,1,0:T(8,128)(2,1)} %param.16) | copy-start | bytes 3145732
  8.0 44.5 %copy-start.14 = (f32[2048]{0:T(1024)S(1)}, f32[2048]{0:T(1024)}, u32[]{:S(2)}) copy-start(f32[2048]{0:T(1024)} %param.17) | copy-start | bytes 24580
  8.0 99.7 %all-gather.12.cloned.1.call-start = ((), (), s32[]{:S(2)}) async-start(), calls=%async_computation.4 | async-start | bytes 1179648 | tf_op jit(solution)/shard_map/all_gather | solution.py:133
  31.4 23.6 %copy-start.10 = (f32[512]{0:T(512)S(1)}, f32[512]{0:T(512)}, u32[]{:S(2)}) copy-start(f32[512]{0:T(512)} %param.21) | copy-start | bytes 6148
  31.4 25.1 %copy-start.7 = (bf16[64,256]{1,0:T(8,128)(2,1)S(1)}, bf16[64,256]{1,0:T(8,128)(2,1)}, u32[]{:S(2)}) copy-start(bf16[64,256]{1,0:T(8,128)(2,1)} %param.24) | copy-start | bytes 98308
  31.4 113.8 %all-gather.8.cloned.1.call-start = ((), (), s32[]{:S(2)}) async-start(), calls=%async_computation.2 | async-start | bytes 2359296 | tf_op jit(solution)/shard_map/all_gather | solution.py:132
  55.0 38.8 %copy-start.6 = (bf16[128,384]{1,0:T(8,128)(2,1)S(1)}, bf16[128,384]{1,0:T(8,128)(2,1)}, u32[]{:S(2)}) copy-start(bf16[128,384]{1,0:T(8,128)(2,1)} %param.23) | copy-start | bytes 294916
  55.8 46.3 %copy-start.8 = (bf16[64,256]{1,0:T(8,128)(2,1)S(1)}, bf16[64,256]{1,0:T(8,128)(2,1)}, u32[]{:S(2)}) copy-start(bf16[64,256]{1,0:T(8,128)(2,1)} %param.25) | copy-start | bytes 98308
  55.9 196.1 %all-gather.14.cloned.1.call-start = ((), (), s32[]{:S(2)}) async-start(), calls=%async_computation.5 | async-start | bytes 8650752 | tf_op jit(solution)/shard_map/all_gather | solution.py:151
  109.4 0.7 copy-start.12
  110.7 1.6 copy-start.1
  147.9 0.7 copy-start.13
  149.2 1.0 copy-start.3
  149.2 1.0 copy-start.4
  150.5 1.2 copy-start.2
  249.3 2.2 copy-start.9
Sparse Core Ops, SparseCore 0:
  8.9 19.4 all-gather.9
  29.9 22.5 all-gather.5
  54.6 40.9 all-gather.11
  97.6 47.5 all-gather.7
  147.9 75.5 all-gather.13
where the time goes:
time: 266 us; the launch traced here: 265 us
  blocking collectives  77.4 us (29%)
  waiting for transfers between devices  71 us (27%)
  matrix products  70.4 us (26%)
  local copies, waits for them, and re-layouts  16.9 us (6%)
  between operations  13.4 us (5%)
  other arithmetic  13.3 us (5%)
    sub x4, matrix products, one_block(): weights = jax.nn.softmax(scores, axis=-1).astype(jnp.bfloat16)  32.8 us
    all_gather x1, blocking collectives, per_device(): lax.all_gather(rope_key, 'sp', axis=0, tiled=True)  31.3 us
    all_gather x1, waiting for transfers between devices, per_device(): lax.all_gather(latent_q, 'sp', axis=0, tiled=True)  29.2 us
    all_to_all x1, blocking collectives, per_device(): lax.all_to_all(attended, 'sp', split_axis=0, concat_axis=1, tiled=True)  28.6 us
    all_gather x1, waiting for transfers between devices, per_device(): lax.all_gather(w_query_down, 'dp', axis=0, tiled=True)  21.1 us
    dot_general x4, matrix products, one_block(): jnp.einsum('hqk,khd->qhd', weights, value_heads, preferred_element_type=j...  19.9 us
    all_gather x1, waiting for transfers between devices, per_device(): lax.all_gather(w_latent_down, 'dp', axis=0, tiled=True)  18.7 us
    dot_general x2, matrix products, single_fold(): return jnp.dot(inputs, piece, preferred_element_type=jnp.float32)  9.36 us
  transfers between devices with their start and end apart: 5, of which 3 were waited for; matrix products, arithmetic and copies ran while one was open for 34% of the time, Pallas kernels for 0%

commit v1 on v0

v1 whole, which is shorter than its diff:
```python
import functools

import jax
import jax.numpy as jnp
from jax import lax
from jax.experimental import pallas as pl
from jax.experimental.pallas import tpu as pltpu
from jax.sharding import PartitionSpec as P

HEADS = 16
EPS = 1e-06
THETA = 10000.0
NEG_BIG = -1e30
LOG2E = 1.4426950408889634
NT = (((1,), (1,)), ((), ()))


def rms_scale(values, scaling):
    return values * lax.rsqrt(jnp.mean(values * values, axis=-1, keepdims=True) + EPS) * scaling


def swap_halves(x):
    half = x.shape[-1] // 2
    return jnp.concatenate([x[..., half:], x[..., :half]], axis=-1)


def tables(length, width, gains):
    half = width // 2
    frequency = THETA ** (-jnp.arange(half, dtype=jnp.float32) / half)
    angles = jnp.arange(length, dtype=jnp.float32)[:, None] * frequency[None, :]
    cosine, sine = jnp.cos(angles), jnp.sin(angles)
    base = jnp.concatenate([cosine, cosine, -sine, sine], axis=-1)
    out = []
    for gain in gains:
        tail = gain[-width:]
        out.append(base * jnp.concatenate([tail, swap_halves(tail)])[None, :])
    return out


def widen_query(w, head_count, rope):
    rows = w.shape[0]
    w = w.reshape(rows, head_count, -1)
    return jnp.concatenate([w, swap_halves(w[..., -rope:])], axis=-1).reshape(rows, -1)


def project_block(i, rows, heads, nope, vd, lq, lkv, rp, wq, wk, wvt, gq, gk, tq, tk, q_s, k_s, v_s):
    tok = pl.ds(pl.multiple_of(i * rows, rows), rows)
    wide = wq.shape[1] // heads
    rope2 = wide - nope
    inv = 1.0 / (nope + rope2 // 2)
    q = jnp.dot(lq, wq[...], preferred_element_type=jnp.float32)
    k = jnp.dot(lkv, wk[...], preferred_element_type=jnp.float32)
    v_s[:, tok] = lax.dot_general(wvt[...], lkv, NT, preferred_element_type=jnp.float32).astype(jnp.bfloat16)
    shared = rp.astype(jnp.float32)
    shared_sq = 0.5 * shared * shared
    lane = lax.broadcasted_iota(jnp.int32, (rows, rope2), 1)
    tqv, tkv = tq[tok, :], tk[tok, :]
    for h in range(heads):
        for which in range(2):
            if which == 0:
                t1 = q[:, h * wide : h * wide + nope]
                t2 = q[:, h * wide + nope : (h + 1) * wide]
                sq, gain, table, dest = t1 * t1 + 0.5 * t2 * t2, gq, tqv, q_s
            else:
                t1, t2 = k[:, h * nope : (h + 1) * nope], shared
                sq, gain, table, dest = t1 * t1 + shared_sq, gk, tkv, k_s
            r = lax.rsqrt(jnp.sum(sq, axis=-1, keepdims=True) * inv + EPS)
            dest[h, tok, 0:nope] = (t1 * r * gain[...]).astype(jnp.bfloat16)
            y = t2 * r * table
            y = y + pltpu.roll(y, rope2 // 2, 1)
            if which == 1:
                y = jnp.where(lane < rope2 // 2, y, 0.0)
            dest[h, tok, nope:wide] = y.astype(jnp.bfloat16)


def attend_block(qb, rows, chunk, heads, vd, scale, q_s, k_s, v_s):
    qtok = pl.ds(pl.multiple_of(qb * rows, rows), rows)
    qs = [q_s[h, qtok, :] for h in range(heads)]
    factor = scale * LOG2E

    def step(kb, carry, masked):
        ktok = pl.ds(pl.multiple_of(kb * chunk, chunk), chunk)
        new = []
        for h in range(heads):
            m, l, acc = carry[h]
            s = lax.dot_general(k_s[h, ktok, :], qs[h], NT, preferred_element_type=jnp.float32) * factor
            if masked:
                kpos = kb * chunk + lax.broadcasted_iota(jnp.int32, (chunk, rows), 0)
                qpos = qb * rows + lax.broadcasted_iota(jnp.int32, (chunk, rows), 1)
                s = jnp.where(kpos <= qpos, s, NEG_BIG)
            m_new = jnp.maximum(m, jnp.max(s, axis=0, keepdims=True))
            alpha = jnp.exp2(m - m_new)
            p = jnp.exp2(s - m_new)
            l = l * alpha + jnp.sum(p, axis=0, keepdims=True)
            vt = v_s[h * vd : (h + 1) * vd, ktok]
            acc = acc * alpha + jnp.dot(vt, p.astype(jnp.bfloat16), preferred_element_type=jnp.float32)
            new.append((m_new, l, acc))
        return tuple(new)

    carry = tuple(
        (
            jnp.full((1, rows), NEG_BIG, jnp.float32),
            jnp.zeros((1, rows), jnp.float32),
            jnp.zeros((vd, rows), jnp.float32),
        )
        for _ in range(heads)
    )
    last = (qb * rows) // chunk
    carry = lax.fori_loop(0, last, lambda kb, c: step(kb, c, False), carry)
    carry = step(last, carry, True)
    return jnp.concatenate([jnp.transpose(acc / l) for _, l, acc in carry], axis=1).astype(jnp.bfloat16)


def attention_kernel(
    blocks, rows, chunk, heads, nope, vd, scale,
    lq, lkv, rp, wq, wk, wvt, gq, gk, tq, tk, out, q_s, k_s, v_s,
):
    def project(i, _):
        tok = pl.ds(pl.multiple_of(i * rows, rows), rows)
        project_block(
            i, rows, heads, nope, vd, lq[tok, :], lkv[tok, :], rp[tok, :],
            wq, wk, wvt, gq, gk, tq, tk, q_s, k_s, v_s,
        )
        return 0

    lax.fori_loop(0, blocks, project, 0)

    def attend(qb, _):
        tok = pl.ds(pl.multiple_of(qb * rows, rows), rows)
        out[tok, :] = attend_block(qb, rows, chunk, heads, vd, scale, q_s, k_s, v_s)
        return 0

    lax.fori_loop(0, blocks, attend, 0)


def per_device(
    tokens, in_gain, w_query_down, w_latent_down, w_rope_key, query_latent_gain, latent_gain,
    w_query_up, w_key_up, w_value_up, query_gain, key_gain, out_gain, w_out,
):
    seq_devices = lax.axis_size("sp")
    heads = HEADS // seq_devices
    own_rows = tokens.shape[1]
    length = own_rows * seq_devices
    rope = w_rope_key.shape[1]
    nope = w_key_up.shape[1] // heads
    vd = w_value_up.shape[1] // heads
    qk = nope + rope
    qr, kr = w_query_down.shape[1], w_latent_down.shape[1]
    out_full = lax.all_gather(w_out, ("sp", "dp"), axis=0, tiled=True)
    local_rows = tokens.reshape(own_rows, tokens.shape[2])
    normed = rms_scale(local_rows.astype(jnp.float32), in_gain).astype(jnp.bfloat16)
    down = lax.all_gather(
        jnp.concatenate([w_query_down, w_latent_down], axis=1), "dp", axis=0, tiled=True
    )
    sums = jnp.dot(normed, down, preferred_element_type=jnp.float32)
    latent_q = rms_scale(sums[:, :qr], query_latent_gain).astype(jnp.bfloat16)
    latent_kv = rms_scale(sums[:, qr:], latent_gain).astype(jnp.bfloat16)
    wide_rope = jnp.concatenate([w_rope_key, swap_halves(w_rope_key)], axis=1)
    rope_key = jnp.dot(normed, wide_rope, preferred_element_type=jnp.float32).astype(jnp.bfloat16)
    lat = lax.all_gather(
        jnp.concatenate([latent_q, latent_kv, rope_key], axis=1), "sp", axis=0, tiled=True
    )
    wq = lax.all_gather(w_query_up, "dp", axis=0, tiled=True)
    wkv = lax.all_gather(jnp.concatenate([w_key_up, w_value_up], axis=1), "dp", axis=0, tiled=True)
    wk, wv = wkv[:, : heads * nope], wkv[:, heads * nope :]
    tq, tk = tables(length, rope, (query_gain, key_gain))
    chunk = min(2 * own_rows, length)
    attended = pl.pallas_call(
        functools.partial(
            attention_kernel, seq_devices, own_rows, chunk, heads, nope, vd, float(qk) ** -0.5
        ),
        out_shape=jax.ShapeDtypeStruct((length, heads * vd), jnp.bfloat16),
        scratch_shapes=[
            pltpu.VMEM((heads, length, qk + rope), jnp.bfloat16),
            pltpu.VMEM((heads, length, qk + rope), jnp.bfloat16),
            pltpu.VMEM((heads * vd, length), jnp.bfloat16),
        ],
        compiler_params=pltpu.CompilerParams(vmem_limit_bytes=56 * 1024 * 1024),
        cost_estimate=pl.CostEstimate(flops=8 * 10**9, bytes_accessed=10**7, transcendentals=5 * 10**6),
    )(
        lat[:, :qr], lat[:, qr : qr + kr], lat[:, qr + kr :],
        widen_query(wq, heads, rope), wk, wv.T,
        query_gain[None, :nope], key_gain[None, :nope], tq, tk,
    )
    token_heads = lax.all_to_all(attended, "sp", split_axis=0, concat_axis=1, tiled=True)
    mixed = rms_scale(token_heads.astype(jnp.float32), out_gain).astype(jnp.bfloat16)
    projected = jnp.dot(mixed, out_full, preferred_element_type=jnp.float32)
    return projected.astype(jnp.bfloat16).reshape(1, own_rows, w_out.shape[1])


def solution(mesh):
    in_specs = (
        P("dp", "sp", None), P(), P("dp", None), P("dp", None), P(), P(), P(),
        P("dp", "sp"), P("dp", "sp"), P("dp", "sp"), P(), P(), P(), P(("sp", "dp"), None),
    )
    return jax.shard_map(
        per_device, mesh=mesh, in_specs=in_specs, out_specs=P("dp", "sp", None), check_vma=False
    )
```

time: 266 us -> 220 us (0.83)
  matrix products: 70.4 us -> 10.1 us
  Pallas kernels: 0 us -> 33 us
  blocking collectives: 77.4 us -> 62.5 us
  waiting for transfers between devices: 71 us -> 77.4 us
  local copies, waits for them, and re-layouts: 16.9 us -> 12.1 us
  other arithmetic: 13.3 us -> 10.6 us
    all_gather x4 -> x2, blocking collectives: 48.9 us -> 12.3 us  [the longest x1 6.49 us: per_device(): wq = lax.all_gather(w_query_up, 'dp', axis=0, tiled=True)]
    pallas_call x0 -> x1, Pallas kernels: none -> 33 us  [per_device(): pl.pallas_call(functools.partial(attention_kernel, seq_devices, own_rows,...]
    sub x4 -> x0, matrix products: 32.8 us -> none  [one_block(): weights = jax.nn.softmax(scores, axis=-1).astype(jnp.bfloat16)]
    dot_general x11 -> x3, matrix products: 37.6 us -> 10.1 us  [the longest x1 6.7 us: per_device(): projected = jnp.dot(mixed, out_full, preferred_element_type=jnp.float32)]
    all_to_all x1, blocking collectives: 28.6 us -> 50.2 us  [per_device(): lax.all_to_all(attended, 'sp', split_axis=0, concat_axis=1, tiled=True)]
    all_gather x5 -> x3, waiting for transfers between devices: 69 us -> 76.6 us  [the longest x1 43.7 us: per_device(): lax.all_gather(jnp.concatenate([latent_q, latent_kv, rope_key], axis=1),...]
    slice x2 -> x10, local copies, waits for them, and re-layouts: 1.3 us -> 8.1 us  [the longest x1 3.1 us: per_device(): lat[:, :qr]]
    unnamed x31 -> x24, local copies, waits for them, and re-layouts: 5.17 us -> 0.93 us
  transfers between devices with their start and end apart: 5 -> 3, of which waited for: 3 -> 3; matrix products, arithmetic and copies ran while one was open for 34% -> 9% of each run, Pallas kernels for 0% -> 15%
where the time goes in v1:
time: 220 us; the launch traced here: 219 us
  waiting for transfers between devices  77.4 us (35%)
  blocking collectives  62.5 us (28%)
  Pallas kernels  33 us (15%)
  between operations  13.3 us (6%)
  local copies, waits for them, and re-layouts  12.1 us (6%)
  other arithmetic  10.6 us (5%)
  matrix products  10.1 us (5%)
    all_to_all x1, blocking collectives, per_device(): lax.all_to_all(attended, 'sp', split_axis=0, concat_axis=1, tiled=True)  50.2 us
    all_gather x1, waiting for transfers between devices, per_device(): lax.all_gather(jnp.concatenate([latent_q, latent_kv, rope_key], axis=1),...  43.7 us
    pallas_call x1, Pallas kernels, per_device(): pl.pallas_call(functools.partial(attention_kernel, seq_devices, own_rows,...  33 us
    all_gather x1, waiting for transfers between devices, per_device(): lax.all_gather(jnp.concatenate([w_query_down, w_latent_down], axis=1), 'd...  30.5 us
    dot_general x1, matrix products, per_device(): projected = jnp.dot(mixed, out_full, preferred_element_type=jnp.float32)  6.7 us
    all_gather x1, blocking collectives, per_device(): wq = lax.all_gather(w_query_up, 'dp', axis=0, tiled=True)  6.49 us
    all_gather x1, blocking collectives, per_device(): lax.all_gather(jnp.concatenate([w_key_up, w_value_up], axis=1), 'dp', axi...  5.85 us
  transfers between devices with their start and end apart: 3, of which 3 were waited for; matrix products, arithmetic and copies ran while one was open for 9% of the time, Pallas kernels for 15%

profile of v1, /device:TPU:0, one launch (start us, length us, event | category | flops | bytes accessed | tf_op | source)
XLA Modules:
  0.0 219.2 jit_solution(16894680069019547287)
XLA Ops:
  6.5 2.2 pad_maximum_fusion.1
  8.8 0.3 fusion.1
  9.1 0.5 convolution_convert_fusion.1
  9.7 30.5 %all-gather.4.cloned.1.call-done = bf16[2048,768]{1,0:T(8,128)(2,1)} async-done(((bf16[512,768]{1,0:T(8,128)(2,1)}), bf16[2048,768]{1,0:T(8,128)(2,1)}) %all-gather.4.cloned.1.call-update) | async-done | bytes 3145744 | tf_op jit(solution)/shard_map/all_gather | solution.py:152
  40.2 2.9 %fusion.15 = f32[256,768]{1,0:T(8,128)S(1)} fusion(bf16[2048,768]{1,0:T(8,128)(2,1)} %all-gather.4.cloned.1.call-done, bf16[1,256,2048]{2,1,0:T(8,128)(2,1)S(1)} %copy-done, f32[2048]{0:T(1024)S(1)} %copy-done.10, f32[256]{0:T(256)S(1)} %add_rsqrt_fusion.3), kind=kOutput, calls=%fused_computation.29 | convolution fusion | flops 807403520 | bytes 4989952 | tf_op jit(solution)/shard_map/dot_general | solution.py:155
  43.1 0.1 multiply_reduce_fusion.1
  43.2 0.1 multiply_reduce_fusion.2
  43.4 0.1 multiply_convert_fusion
  43.5 0.1 multiply_convert_fusion.1
  43.6 0.8 pad_maximum_fusion.3
  44.5 0.7 all-gather.8.cloned.1.call-update
  45.3 0.1 copy.32
  45.4 6.5 %all_gather.17 = bf16[512,384]{0,1:T(8,128)(2,1)S(1)} all-gather(bf16[128,384]{0,1:T(8,128)(2,1)S(1)} %copy.32), channel_id=1, replica_groups=mesh['sp'=8,'dp'=4] {'dp'}, dimensions={0}, use_global_device_ids=true | all-gather | bytes 491520 | tf_op jit(solution)/shard_map/all_gather | solution.py:163
  51.9 1.0 copy.38.wq
  53.0 5.9 %all_gather.18 = bf16[256,512]{1,0:T(8,128)(2,1)S(1)} all-gather(bf16[64,512]{1,0:T(8,128)(2,1)S(1)} %pad_maximum_fusion.4), channel_id=1, replica_groups=mesh['sp'=8,'dp'=4] {'dp'}, dimensions={0}, use_global_device_ids=true | all-gather | bytes 327680 | tf_op jit(solution)/shard_map/all_gather | solution.py:164
  58.8 0.7 fusion.19
  59.5 0.8 copy.39
  60.4 0.1 pad_maximum_fusion.5
  60.5 0.6 slice_bitcast_fusion
  61.0 3.9 %fusion.7 = (f32[2048,32]{1,0:T(8,128)S(1)}, f32[2048,32]{1,0:T(8,128)S(1)}, f32[2048,32]{1,0:T(8,128)S(1)}) fusion(f32[32]{0:T(128)S(1)} %multiply_power_fusion), kind=kLoop, calls=%fused_computation.15 | loop fusion | flops 131072 | bytes 786560 | tf_op jit(solution)/shard_map/cos | solution.py:31
  64.9 2.2 %broadcast_multiply_fusion = (f32[2048,128]{1,0:T(8,128)}, f32[2048,128]{1,0:T(8,128)}) fusion(f32[128]{0:T(128)S(1)} %get-tuple-element.21, f32[2048,32]{1,0:T(8,128)S(1)} %get-tuple-element.19, f32[2048,32]{1,0:T(8,128)S(1)} %get-tuple-element.18, f32[2048,32]{1,0:T(8,128)S(1)} %get-tuple-element.17, f32[128]{0:T(128)S(1)} %get-tuple-element.20), kind=kLoop, calls=%fused_computation.23 | loop fusion | flops 1310720 | bytes 2884608 | tf_op jit(solution)/shard_map/mul | solution.py:36
  67.2 43.7 %all-gather.6.cloned.1.call-done = bf16[2048,896]{1,0:T(8,128)(2,1)} async-done(((bf16[256,896]{1,0:T(8,128)(2,1)}), bf16[2048,896]{1,0:T(8,128)(2,1)}) %all-gather.6.cloned.1.call-update) | async-done | bytes 3670032 | tf_op jit(solution)/shard_map/all_gather | solution.py:160
  110.8 3.1 %slice.85.lq = bf16[2048,512]{1,0:T(8,128)(2,1)} slice(bf16[2048,896]{1,0:T(8,128)(2,1)} %all-gather.6.cloned.1.call-done), slice={[0:2048], [0:512]} | slice | bytes 4194304 | tf_op jit(solution)/shard_map/slice | solution.py:181
  113.9 2.3 %slice.86.lkv = bf16[2048,256]{1,0:T(8,128)(2,1)} slice(bf16[2048,896]{1,0:T(8,128)(2,1)} %all-gather.6.cloned.1.call-done), slice={[0:2048], [512:768]} | slice | bytes 2097152 | tf_op jit(solution)/shard_map/slice | solution.py:181
  116.2 1.9 slice.87.rp
  118.1 33.0 %shard_map.136 = bf16[2048,256]{1,0:T(8,128)(2,1)} custom-call(bf16[2048,512]{1,0:T(8,128)(2,1)} %slice.85.lq, bf16[2048,256]{1,0:T(8,128)(2,1)} %slice.86.lkv, bf16[2048,128]{1,0:T(8,128)(2,1)} %slice.87.rp, bf16[512,512]{1,0:T(8,128)(2,1)} %copy.38.wq, bf16[256,256]{1,0:T(8,128)(2,1)} %get-tuple-element.10.wk, bf16[256,256]{1,0:T(8,128)(2,1)} %bitcast.31, ...), custom_call_target="tpu_custom_call" | custom-call | flops 8000000000 | bytes 10000000 | tf_op jit(solution)/shard_map/pallas_call | solution.py:168
  151.1 1.5 copy.36
  152.6 50.2 %all_to_all.13 = bf16[8,256,256]{1,2,0:T(8,128)(2,1)S(1)} all-to-all(bf16[8,256,256]{1,2,0:T(8,128)(2,1)S(1)} %copy.36), channel_id=1, replica_groups=mesh['sp'=8,'dp'=4] {'sp'}, dimensions={0} | all-to-all | bytes 2097152 | tf_op jit(solution)/shard_map/all_to_all | solution.py:185
  202.8 0.3 multiply_reduce_fusion
  203.1 0.3 fusion.5
  203.5 2.5 %all-gather.8.cloned.1.call-done = bf16[2048,2048]{1,0:T(8,128)(2,1)} async-done(((bf16[64,2048]{1,0:T(8,128)(2,1)}), bf16[2048,2048]{1,0:T(8,128)(2,1)}) %all-gather.8.cloned.1.call-update) | async-done | bytes 8388624 | tf_op jit(solution)/shard_map/all_gather | solution.py:149
  206.0 6.7 %fusion = bf16[1,256,2048]{2,1,0:T(8,128)(2,1)} fusion(bf16[256,2048]{0,1:T(8,128)(2,1)S(1)} %fusion.5, bf16[2048,2048]{1,0:T(8,128)(2,1)} %all-gather.8.cloned.1.call-done), kind=kOutput, calls=%fused_computation.3 | convolution fusion | flops 2148007936 | bytes 10485760 | tf_op jit(solution)/shard_map/dot_general | solution.py:187
  (40 shorter events, 0.4 us)
Async XLA Ops:
  6.5 2.2 %copy-start = (bf16[1,256,2048]{2,1,0:T(8,128)(2,1)S(1)}, bf16[1,256,2048]{2,1,0:T(8,128)(2,1)}, u32[]{:S(2)}) copy-start(bf16[1,256,2048]{2,1,0:T(8,128)(2,1)} %param.14) | copy-start | bytes 3145732
  6.5 2.5 %copy-start.1 = (bf16[2048,64]{0,1:T(8,128)(2,1)S(1)}, bf16[2048,64]{0,1:T(8,128)(2,1)}, u32[]{:S(2)}) copy-start(bf16[2048,64]{0,1:T(8,128)(2,1)} %param.18) | copy-start | bytes 786436
  6.5 2.6 %copy-start.10 = (f32[2048]{0:T(1024)S(1)}, f32[2048]{0:T(1024)}, u32[]{:S(2)}) copy-start(f32[2048]{0:T(1024)} %param.15) | copy-start | bytes 24580
  6.5 33.6 %all-gather.4.cloned.1.call-start = ((), (), s32[]{:S(2)}) async-start(), calls=%async_computation.1 | async-start | bytes 3932160 | tf_op jit(solution)/shard_map/all_gather | solution.py:152
  8.7 102.1 %all-gather.6.cloned.1.call-start = ((), (), s32[]{:S(2)}) async-start(), calls=%async_computation.2 | async-start | bytes 4128768 | tf_op jit(solution)/shard_map/all_gather | solution.py:160
  9.6 33.8 %copy-start.8 = (f32[512]{0:T(512)S(1)}, f32[512]{0:T(512)}, u32[]{:S(2)}) copy-start(f32[512]{0:T(512)} %param.19) | copy-start | bytes 6148
  9.6 33.9 %copy-start.9 = (f32[256]{0:T(256)S(1)}, f32[256]{0:T(256)}, u32[]{:S(2)}) copy-start(f32[256]{0:T(256)} %param.20) | copy-start | bytes 3076
  43.1 2.1 copy-start.7
  43.1 2.1 copy-start.6
  43.1 2.1 copy-start.2
  44.4 8.5 %copy-start.3 = (bf16[64,256]{1,0:T(8,128)(2,1)S(1)}, bf16[64,256]{1,0:T(8,128)(2,1)}, u32[]{:S(2)}) copy-start(bf16[64,256]{1,0:T(8,128)(2,1)} %param.23) | copy-start | bytes 98308
  44.4 8.5 %copy-start.4 = (bf16[64,256]{1,0:T(8,128)(2,1)S(1)}, bf16[64,256]{1,0:T(8,128)(2,1)}, u32[]{:S(2)}) copy-start(bf16[64,256]{1,0:T(8,128)(2,1)} %param.22) | copy-start | bytes 98308
  44.5 161.5 %all-gather.8.cloned.1.call-start = ((), (), s32[]{:S(2)}) async-start(), calls=%async_computation.3 | async-start | bytes 8650752 | tf_op jit(solution)/shard_map/all_gather | solution.py:149
  152.6 50.5 %copy-start.5 = (f32[2048]{0:T(1024)S(1)}, f32[2048]{0:T(1024)}, u32[]{:S(2)}) copy-start(f32[2048]{0:T(1024)} %param.26) | copy-start | bytes 24580
Sparse Core Ops, SparseCore 0:
  8.9 31.2 all-gather.3
  44.6 66.2 all-gather.5
  113.7 92.1 all-gather.7

commit v2 on v1

--- a/solution.py
+++ b/solution.py
@@ -111,81 +111,297 @@
     return jnp.concatenate([jnp.transpose(acc / l) for _, l, acc in carry], axis=1).astype(jnp.bfloat16)
 
 
-def attention_kernel(
-    blocks, rows, chunk, heads, nope, vd, scale,
-    lq, lkv, rp, wq, wk, wvt, gq, gk, tq, tk, out, q_s, k_s, v_s,
+MESH = pl.DeviceIdType.MESH
+
+
+class Links:
+    def __init__(self, send_sems, recv_sems):
+        self.send_sems, self.recv_sems, self.ids, self.sent = send_sems, recv_sems, {}, []
+
+    def copy(self, role, src, dst, target):
+        n = self.ids.setdefault(role, len(self.ids))
+        return pltpu.make_async_remote_copy(
+            src_ref=src, dst_ref=dst, send_sem=self.send_sems.at[n], recv_sem=self.recv_sems.at[n],
+            device_id=target, device_id_type=MESH,
+        )
+
+    def send(self, role, src, dst, target, ok=None):
+        self.sent.append((ok, role, src, dst, target))
+        guard(ok, lambda: self.copy(role, src, dst, target).start())
+
+    def arrive(self, role, dst, target, ok=None):
+        guard(ok, lambda: self.copy(role, dst, dst, target).wait_recv())
+
+    def drain(self):
+        for ok, role, src, dst, target in self.sent:
+            guard(ok, lambda: self.copy(role, src, dst, target).wait_send())
+        self.sent = []
+
+
+def guard(ok, action):
+    if ok is None:
+        action()
+    else:
+        pl.when(ok)(action)
+
+
+def sem_count(nx, ny, nz, cores):
+    gather = 4 * ((nx - 1) * cores + cores - 1) + 2 * (nx - 1) * (ny - 1) * cores
+    latent = 2 * (2 * (nz - 1) + (2 * nz - 1) * (ny - 1))
+    return gather + latent
+
+
+def layer_kernel(
+    dims, chunk, heads, nope, vd, scale,
+    tokens, in_gain, wqd, wld, wrope, q_lat_gain, kv_lat_gain, wqu, wkvu, gq, gk, tq, tk, out_gain,
+    out,
+    normed, wqd_g, wld_g, wqu_g, wkvu_g, wvt, kvr_g, q_g, q_s, k_s, v_s, att_s, heads_g,
+    send_sems, recv_sems, a2a_send, a2a_recv,
 ):
+    nx, ny, nz, cores = dims
+    seqs, dps = ny * nz, nx * cores
+    rows = tokens.shape[0]
+    kr = wld.shape[1]
+    s, d = lax.axis_index("sp"), lax.axis_index("dp")
+    y, z = lax.rem(s, ny), lax.div(s, ny)
+    c, x = lax.rem(d, cores), lax.div(d, cores)
+    links = Links(send_sems, recv_sems)
+
+    def at_sp(target):
+        return {"sp": target, "dp": d}
+
+    def at_dp(target):
+        return {"sp": s, "dp": target}
+
+    barrier = pltpu.get_barrier_semaphore()
+    for k in range(1, seqs):
+        pl.semaphore_signal(barrier, inc=1, device_id=at_sp(lax.rem(s + k, seqs)), device_id_type=MESH)
+    for k in range(1, dps):
+        pl.semaphore_signal(barrier, inc=1, device_id=at_dp(lax.rem(d + k, dps)), device_id_type=MESH)
+    pl.semaphore_wait(barrier, seqs + dps - 2)
+
+    weights = ((wqd, wqd_g, True), (wld, wld_g, True), (wqu, wqu_g, False), (wkvu, wkvu_g, False))
+
+    def piece(ref, split, which):
+        part = ref.shape[0] // ny
+        return ref.at[pl.ds(pl.multiple_of(which * part, part), part)] if split else ref
+
+    partners = [(dc, x * cores + lax.rem(c + dc, cores)) for dc in range(1, cores)]
+    for a, (src, dst, split) in enumerate(weights):
+        for dx in range(1, nx):
+            target = lax.rem(x + dx, nx) * cores + c
+            links.send(("x", a, dx), piece(src, split, y), piece(dst.at[d], split, y), at_dp(target))
+        for dc, partner in partners:
+            links.send(("c", a, dc), src, dst.at[d], at_dp(partner))
+    for src, dst, _ in weights:
+        dst[d] = src[...]
+
+    def norm(i, _):
+        step = rows // 4
+        band = pl.ds(pl.multiple_of(i * step, step), step)
+        normed[band, :] = rms_scale(tokens[band, :].astype(jnp.float32), in_gain[...]).astype(jnp.bfloat16)
+        return 0
+
+    lax.fori_loop(0, 4, norm, 0)
+
+    for a, (src, dst, split) in enumerate(weights):
+        for dx in range(1, nx):
+            origin = lax.rem(x - dx + nx, nx) * cores + c
+            got = piece(dst.at[origin], split, y)
+            links.arrive(("x", a, dx), got, at_dp(d))
+            for dy in range(1, ny if split else 1):
+                links.send(("y", a, dx, dy), got, got, at_sp(z * ny + lax.rem(y + dy, ny)))
+            for dc, partner in partners:
+                links.send(("cx", a, dx, dc), got, got, at_dp(partner))
+    rope_key = jnp.dot(normed[...], wrope[...], preferred_element_type=jnp.float32)
+    kvr_g[s, :, kr:] = rope_key.astype(jnp.bfloat16)
+    for a, (src, dst, split) in enumerate(weights):
+        for dx in range(1, nx):
+            origin = lax.rem(x - dx + nx, nx) * cores + c
+            for dy in range(1, ny if split else 1):
+                got = piece(dst.at[origin], split, lax.rem(y - dy + ny, ny))
+                links.arrive(("y", a, dx, dy), got, at_dp(d))
+                for dc, partner in partners:
+                    links.send(("cy", a, dx, dy, dc), got, got, at_dp(partner))
+
+    def settle(a):
+        src, dst, split = weights[a]
+        for dc, _ in partners:
+            other = lax.rem(c - dc + cores, cores)
+            links.arrive(("c", a, dc), dst.at[x * cores + other], at_dp(d))
+            for dx in range(1, nx):
+                origin = dst.at[lax.rem(x - dx + nx, nx) * cores + other]
+                links.arrive(("cx", a, dx, dc), piece(origin, split, y), at_dp(d))
+                for dy in range(1, ny if split else 1):
+                    got = piece(origin, split, lax.rem(y - dy + ny, ny))
+                    links.arrive(("cy", a, dx, dy, dc), got, at_dp(d))
+
+    def down(gathered):
+        part = gathered.shape[1]
+        total = None
+        for k in range(dps):
+            term = jnp.dot(
+                normed[:, k * part : (k + 1) * part], gathered[k], preferred_element_type=jnp.float32
+            )
+            total = term if total is None else total + term
+        return total
+
+    buffers = (kvr_g, q_g)
+
+    def over_y(b, tag, slot, ok=None):
+        block = buffers[b].at[slot]
+        for dy in range(1, ny):
+            links.send(("ly", b, tag, dy), block, block, at_sp(z * ny + lax.rem(y + dy, ny)), ok)
+
+    def along_z(b, way, step, slot, ok):
+        block = buffers[b].at[slot]
+        links.send(("z", b, way, step), block, block, at_sp(jnp.clip(z + way, 0, nz - 1) * ny + y), ok)
+
+    def launch(b):
+        over_y(b, 0, s)
+        for way in (1, -1):
+            if nz > 1:
+                along_z(b, way, 0, s, (z + way >= 0) & (z + way < nz))
+
+    settle(1)
+    kvr_g[s, :, :kr] = rms_scale(down(wld_g), kv_lat_gain[...]).astype(jnp.bfloat16)
+    launch(0)
+    settle(0)
+    q_g[s] = rms_scale(down(wqd_g), q_lat_gain[...]).astype(jnp.bfloat16)
+    launch(1)
+
+    for step in range(nz - 1):
+        for b in range(2):
+            for way in (1, -1):
+                origin = z - way * (step + 1)
+                ok = (origin >= 0) & (origin < nz)
+                slot = jnp.clip(origin, 0, nz - 1) * ny + y
+                links.arrive(("z", b, way, step), buffers[b].at[slot], at_sp(s), ok)
+                if step < nz - 2:
+                    along_z(b, way, step + 1, slot, ok & (z + way >= 0) & (z + way < nz))
+                over_y(b, way * (step + 1), slot, ok)
+    settle(2)
+    settle(3)
+    wk_cols = heads * nope
+    wq_full = wqu_g.reshape(dps * wqu.shape[0], wqu.shape[1])
+    wkv_full = wkvu_g.reshape(dps * wkvu.shape[0], wkvu.shape[1])
+    wvt[...] = jnp.transpose(wkv_full[:, wk_cols:].astype(jnp.float32)).astype(jnp.bfloat16)
+    for b in range(2):
+        for tag in range(1 - nz, nz):
+            zz = z - tag
+            ok = None if tag == 0 else (zz >= 0) & (zz < nz)
+            for dy in range(1, ny):
+                slot = jnp.clip(zz, 0, nz - 1) * ny + lax.rem(y - dy + ny, ny)
+                links.arrive(("ly", b, tag, dy), buffers[b].at[slot], at_sp(s), ok)
+
     def project(i, _):
-        tok = pl.ds(pl.multiple_of(i * rows, rows), rows)
         project_block(
-            i, rows, heads, nope, vd, lq[tok, :], lkv[tok, :], rp[tok, :],
-            wq, wk, wvt, gq, gk, tq, tk, q_s, k_s, v_s,
+            i, rows, heads, nope, vd, q_g[i], kvr_g[i, :, :kr], kvr_g[i, :, kr:],
+            wq_full, wkv_full.at[:, :wk_cols], wvt, gq, gk, tq, tk, q_s, k_s, v_s,
         )
         return 0
 
-    lax.fori_loop(0, blocks, project, 0)
-
-    def attend(qb, _):
-        tok = pl.ds(pl.multiple_of(qb * rows, rows), rows)
-        out[tok, :] = attend_block(qb, rows, chunk, heads, vd, scale, q_s, k_s, v_s)
+    lax.fori_loop(0, seqs, project, 0)
+
+    def hand_over(qb):
+        return pltpu.make_async_remote_copy(
+            src_ref=att_s.at[qb], dst_ref=heads_g.at[s], send_sem=a2a_send.at[qb],
+            recv_sem=a2a_recv.at[s], device_id=at_sp(qb), device_id_type=MESH,
+        )
+
+    def attend(i, _):
+        qb = lax.rem(s + 1 + i, seqs)
+        att_s[qb] = attend_block(qb, rows, chunk, heads, vd, scale, q_s, k_s, v_s)
+
+        @pl.when(i < seqs - 1)
+        def _():
+            hand_over(qb).start()
+
         return 0
 
-    lax.fori_loop(0, blocks, attend, 0)
+    lax.fori_loop(0, seqs, attend, 0)
+    heads_g[s] = att_s[s]
+    for k in range(1, seqs):
+        origin = lax.rem(s + k, seqs)
+        pltpu.make_async_remote_copy(
+            src_ref=att_s.at[origin], dst_ref=heads_g.at[origin], send_sem=a2a_send.at[origin],
+            recv_sem=a2a_recv.at[origin], device_id=at_sp(origin), device_id_type=MESH,
+        ).wait()
+    links.drain()
+
+    width = heads * vd
+    square = jnp.zeros((rows, 1), jnp.float32)
+    for k in range(seqs):
+        block = heads_g[k].astype(jnp.float32)
+        square = square + jnp.sum(block * block, axis=-1, keepdims=True)
+    r = lax.rsqrt(square * (1.0 / (seqs * width)) + EPS)
+    for k in range(seqs):
+        cols = slice(k * width, (k + 1) * width)
+        out[:, cols] = (heads_g[k].astype(jnp.float32) * r * out_gain[:, cols]).astype(jnp.bfloat16)
 
 
 def per_device(
     tokens, in_gain, w_query_down, w_latent_down, w_rope_key, query_latent_gain, latent_gain,
     w_query_up, w_key_up, w_value_up, query_gain, key_gain, out_gain, w_out,
 ):
-    seq_devices = lax.axis_size("sp")
-    heads = HEADS // seq_devices
+    seqs, dps = lax.axis_size("sp"), lax.axis_size("dp")
+    cores = 2 if dps % 2 == 0 else 1
+    nx = dps // cores
+    ny = nx if seqs % nx == 0 else 1
+    nz = seqs // ny
+    heads = HEADS // seqs
     own_rows = tokens.shape[1]
-    length = own_rows * seq_devices
+    length = own_rows * seqs
     rope = w_rope_key.shape[1]
     nope = w_key_up.shape[1] // heads
     vd = w_value_up.shape[1] // heads
-    qk = nope + rope
-    qr, kr = w_query_down.shape[1], w_latent_down.shape[1]
+    wide = nope + 2 * rope
     out_full = lax.all_gather(w_out, ("sp", "dp"), axis=0, tiled=True)
-    local_rows = tokens.reshape(own_rows, tokens.shape[2])
-    normed = rms_scale(local_rows.astype(jnp.float32), in_gain).astype(jnp.bfloat16)
-    down = lax.all_gather(
-        jnp.concatenate([w_query_down, w_latent_down], axis=1), "dp", axis=0, tiled=True
+    tq, tk = tables(length, rope, (query_gain, key_gain))
+    wide_rope = jnp.concatenate([w_rope_key, swap_halves(w_rope_key)], axis=1)
+    wqu = widen_query(w_query_up, heads, rope)
+    wkvu = jnp.concatenate([w_key_up, w_value_up], axis=1)
+    chunk = min(2 * own_rows, length)
+    sems = sem_count(nx, ny, nz, cores)
+    b16 = jnp.bfloat16
+
+    def gathered(w):
+        return pltpu.VMEM((dps,) + w.shape, b16)
+
+    mixed = pl.pallas_call(
+        functools.partial(
+            layer_kernel, (nx, ny, nz, cores), chunk, heads, nope, vd, float(nope + rope) ** -0.5
+        ),
+        out_shape=jax.ShapeDtypeStruct((own_rows, seqs * heads * vd), b16),
+        in_specs=[pl.BlockSpec(memory_space=pltpu.VMEM)] * 14,
+        out_specs=pl.BlockSpec(memory_space=pltpu.VMEM),
+        scratch_shapes=[
+            pltpu.VMEM((own_rows, tokens.shape[2]), b16),
+            gathered(w_query_down), gathered(w_latent_down), gathered(wqu), gathered(wkvu),
+            pltpu.VMEM((heads * vd, w_latent_down.shape[1]), b16),
+            pltpu.VMEM((seqs, own_rows, w_latent_down.shape[1] + 2 * rope), b16),
+            pltpu.VMEM((seqs, own_rows, w_query_down.shape[1]), b16),
+            pltpu.VMEM((heads, length, wide), b16),
+            pltpu.VMEM((heads, length, wide), b16),
+            pltpu.VMEM((heads * vd, length), b16),
+            pltpu.VMEM((seqs, own_rows, heads * vd), b16),
+            pltpu.VMEM((seqs, own_rows, heads * vd), b16),
+            pltpu.SemaphoreType.DMA((sems,)),
+            pltpu.SemaphoreType.DMA((sems,)),
+            pltpu.SemaphoreType.DMA((seqs,)),
+            pltpu.SemaphoreType.DMA((seqs,)),
+        ],
+        compiler_params=pltpu.CompilerParams(
+            vmem_limit_bytes=56 * 1024 * 1024, collective_id=0, has_side_effects=True
+        ),
+        cost_estimate=pl.CostEstimate(flops=60 * 10**9, bytes_accessed=10**8, transcendentals=5 * 10**6),
+    )(
+        tokens.reshape(own_rows, tokens.shape[2]), in_gain[None], w_query_down, w_latent_down, wide_rope,
+        query_latent_gain[None], latent_gain[None], wqu, wkvu,
+        query_gain[None, :nope], key_gain[None, :nope], tq, tk, out_gain[None],
     )
-    sums = jnp.dot(normed, down, preferred_element_type=jnp.float32)
-    latent_q = rms_scale(sums[:, :qr], query_latent_gain).astype(jnp.bfloat16)
-    latent_kv = rms_scale(sums[:, qr:], latent_gain).astype(jnp.bfloat16)
-    wide_rope = jnp.concatenate([w_rope_key, swap_halves(w_rope_key)], axis=1)
-    rope_key = jnp.dot(normed, wide_rope, preferred_element_type=jnp.float32).astype(jnp.bfloat16)
-    lat = lax.all_gather(
-        jnp.concatenate([latent_q, latent_kv, rope_key], axis=1), "sp", axis=0, tiled=True
-    )
-    wq = lax.all_gather(w_query_up, "dp", axis=0, tiled=True)
-    wkv = lax.all_gather(jnp.concatenate([w_key_up, w_value_up], axis=1), "dp", axis=0, tiled=True)
-    wk, wv = wkv[:, : heads * nope], wkv[:, heads * nope :]
-    tq, tk = tables(length, rope, (query_gain, key_gain))
-    chunk = min(2 * own_rows, length)
-    attended = pl.pallas_call(
-        functools.partial(
-            attention_kernel, seq_devices, own_rows, chunk, heads, nope, vd, float(qk) ** -0.5
-        ),
-        out_shape=jax.ShapeDtypeStruct((length, heads * vd), jnp.bfloat16),
-        scratch_shapes=[
-            pltpu.VMEM((heads, length, qk + rope), jnp.bfloat16),
-            pltpu.VMEM((heads, length, qk + rope), jnp.bfloat16),
-            pltpu.VMEM((heads * vd, length), jnp.bfloat16),
-        ],
-        compiler_params=pltpu.CompilerParams(vmem_limit_bytes=56 * 1024 * 1024),
-        cost_estimate=pl.CostEstimate(flops=8 * 10**9, bytes_accessed=10**7, transcendentals=5 * 10**6),
-    )(
-        lat[:, :qr], lat[:, qr : qr + kr], lat[:, qr + kr :],
-        widen_query(wq, heads, rope), wk, wv.T,
-        query_gain[None, :nope], key_gain[None, :nope], tq, tk,
-    )
-    token_heads = lax.all_to_all(attended, "sp", split_axis=0, concat_axis=1, tiled=True)
-    mixed = rms_scale(token_heads.astype(jnp.float32), out_gain).astype(jnp.bfloat16)
     projected = jnp.dot(mixed, out_full, preferred_element_type=jnp.float32)
-    return projected.astype(jnp.bfloat16).reshape(1, own_rows, w_out.shape[1])
+    return projected.astype(b16).reshape(1, own_rows, w_out.shape[1])
 
 
 def solution(mesh):

time: 220 us -> 165 us (0.75)
  Pallas kernels: 33 us -> 127 us
  waiting for transfers between devices: 77.4 us -> 0.73 us
  blocking collectives: 62.5 us -> 0 us
  local copies, waits for them, and re-layouts: 12.1 us -> 7.52 us
  matrix products: 10.1 us -> 7.02 us
    pallas_call x1, Pallas kernels: 33 us -> 127 us  [per_device(): pl.pallas_call(functools.partial(layer_kernel, (nx, ny, nz, cores), chunk...]
    all_gather x2 -> x0, waiting for transfers between devices: 74.2 us -> none  [the longest x1 43.7 us: per_device(): lax.all_gather(jnp.concatenate([latent_q, latent_kv, rope_key], axis=1),...]
    all_to_all x1 -> x0, blocking collectives: 50.2 us -> none  [per_device(): lax.all_to_all(attended, 'sp', split_axis=0, concat_axis=1, tiled=True)]
    all_gather x2 -> x0, blocking collectives: 12.3 us -> none  [the longest x1 6.49 us: per_device(): wq = lax.all_gather(w_query_up, 'dp', axis=0, tiled=True)]
    slice x4 -> x0, local copies, waits for them, and re-layouts: 7.92 us -> none  [the longest x1 3.1 us: per_device(): lat[:, :qr]]
    dot_general x2 -> x0, matrix products: 3.42 us -> none  [the longest x1 2.92 us: per_device(): sums = jnp.dot(normed, down, preferred_element_type=jnp.float32)]
    all_gather x1, waiting for transfers between devices: 2.47 us -> 0.02 us  [per_device(): out_full = lax.all_gather(w_out, ('sp', 'dp'), axis=0, tiled=True)]
  transfers between devices with their start and end apart: 3 -> 1, of which waited for: 3 -> 0; matrix products, arithmetic and copies ran while one was open for 9% -> 10% of each run, Pallas kernels for 15% -> 77%
where the time goes in v2:
time: 165 us
  Pallas kernels  127 us (77%)
  between operations  13.4 us (8%)
  other arithmetic  8.88 us (5%)
  local copies, waits for them, and re-layouts  7.52 us (5%)
  matrix products  7.02 us (4%)
    pallas_call x1, Pallas kernels, per_device(): pl.pallas_call(functools.partial(layer_kernel, (nx, ny, nz, cores), chunk...  127 us
    dot_general x1, matrix products, per_device(): projected = jnp.dot(mixed, out_full, preferred_element_type=jnp.float32)  7.02 us
    cos x1, other arithmetic, tables(): cosine, sine = (jnp.cos(angles), jnp.sin(angles))  3.89 us
  transfers between devices with their start and end apart: 1, of which 0 were waited for; matrix products, arithmetic and copies ran while one was open for 10% of the time, Pallas kernels for 77%

profile of v2, /device:TPU:0, one launch (start us, length us, event | category | flops | bytes accessed | tf_op | source)
XLA Modules:
  0.0 164.9 jit_solution(9326891994785966973)
XLA Ops:
  6.5 0.0 all-gather.2.cloned.1.call-start
  6.5 0.7 all-gather.2.cloned.1.call-update
  7.3 0.7 slice.49
  7.9 0.7 slice.52
  8.6 1.2 copy.25
  9.8 1.0 copy.26
  10.9 0.8 copy.29.wqu
  11.7 0.8 fusion.6
  12.5 0.8 fusion.7
  13.3 0.1 pad_maximum_fusion.4
  13.4 1.4 pad_maximum_fusion.3.wkvu
  14.8 1.3 slice_bitcast_fusion
  16.1 0.2 fusion.4
  16.3 1.3 pad_maximum_fusion.1.wrope
  17.6 3.9 %fusion.2 = (f32[2048,32]{1,0:T(8,128)S(1)}, f32[2048,32]{1,0:T(8,128)S(1)}, f32[2048,32]{1,0:T(8,128)S(1)}) fusion(f32[32]{0:T(128)S(1)} %multiply_power_fusion), kind=kLoop, calls=%fused_computation.5 | loop fusion | flops 131072 | bytes 786560 | tf_op jit(solution)/shard_map/cos | solution.py:31
  21.5 2.2 %broadcast_multiply_fusion = (f32[2048,128]{1,0:T(8,128)}, f32[2048,128]{1,0:T(8,128)}) fusion(f32[128]{0:T(128)S(1)} %get-tuple-element.19, f32[2048,32]{1,0:T(8,128)S(1)} %get-tuple-element.17, f32[2048,32]{1,0:T(8,128)S(1)} %get-tuple-element.16, f32[2048,32]{1,0:T(8,128)S(1)} %get-tuple-element.15, f32[128]{0:T(128)S(1)} %get-tuple-element.18), kind=kLoop, calls=%fused_computation.7 | loop fusion | flops 1310720 | bytes 2884608 | tf_op jit(solution)/shard_map/mul | solution.py:36
  23.7 127.3 %shard_map.136 = bf16[256,2048]{1,0:T(8,128)(2,1)} custom-call(bf16[256,2048]{1,0:T(8,128)(2,1)} %bitcast.18, f32[1,2048]{1,0:T(1,128)} %bitcast.19, bf16[512,512]{1,0:T(8,128)(2,1)} %wqd.1, bf16[512,256]{1,0:T(8,128)(2,1)} %wld.1, bf16[2048,128]{1,0:T(8,128)(2,1)} %pad_maximum_fusion.1.wrope, f32[1,512]{1,0:T(1,128)} %bitcast.21, f32[1,256]{1,0:T(1,128)} %bitcast.22, ...), custom_call_target="tpu_custom_call" | custom-call | flops 60000002048 | bytes 100000000 | tf_op jit(solution)/shard_map/pallas_call | solution.py:371
  151.0 0.0 all-gather.2.cloned.1.call-done
  151.0 7.0 %fusion = bf16[1,256,2048]{2,1,0:T(8,128)(2,1)} fusion(bf16[256,2048]{1,0:T(8,128)(2,1)} %shard_map.136, bf16[2048,2048]{1,0:T(8,128)(2,1)} %all-gather.2.cloned.1.call-done), kind=kOutput, calls=%fused_computation.1 | convolution fusion | flops 2148007936 | bytes 10485760 | tf_op jit(solution)/shard_map/dot_general | solution.py:403
  (3 shorter events, 0.0 us)
Async XLA Ops:
  6.5 144.5 %all-gather.2.cloned.1.call-start = ((), (), s32[]{:S(2)}) async-start(), calls=%async_computation | async-start | bytes 8650752 | tf_op jit(solution)/shard_map/all_gather | solution.py:359
Sparse Core Ops, SparseCore 0:
  10.2 103.3 all-gather.1

commit v3 on v2

--- a/solution.py
+++ b/solution.py
@@ -2,6 +2,7 @@
 
 import jax
 import jax.numpy as jnp
+import numpy as np
 from jax import lax
 from jax.experimental import pallas as pl
 from jax.experimental.pallas import tpu as pltpu
@@ -24,26 +25,19 @@
     return jnp.concatenate([x[..., half:], x[..., :half]], axis=-1)
 
 
-def tables(length, width, gains):
+def rotation_table(length, width):
     half = width // 2
-    frequency = THETA ** (-jnp.arange(half, dtype=jnp.float32) / half)
-    angles = jnp.arange(length, dtype=jnp.float32)[:, None] * frequency[None, :]
-    cosine, sine = jnp.cos(angles), jnp.sin(angles)
-    base = jnp.concatenate([cosine, cosine, -sine, sine], axis=-1)
-    out = []
-    for gain in gains:
-        tail = gain[-width:]
-        out.append(base * jnp.concatenate([tail, swap_halves(tail)])[None, :])
-    return out
-
-
-def widen_query(w, head_count, rope):
-    rows = w.shape[0]
-    w = w.reshape(rows, head_count, -1)
-    return jnp.concatenate([w, swap_halves(w[..., -rope:])], axis=-1).reshape(rows, -1)
-
-
-def project_block(i, rows, heads, nope, vd, lq, lkv, rp, wq, wk, wvt, gq, gk, tq, tk, q_s, k_s, v_s):
+    frequency = np.float32(THETA) ** (-np.arange(half, dtype=np.float32) / np.float32(half))
+    angles = np.arange(length, dtype=np.float32)[:, None] * frequency[None, :]
+    cosine, sine = np.cos(angles), np.sin(angles)
+    return np.concatenate([cosine, cosine, -sine, sine], axis=-1).astype(np.float32)
+
+
+def with_swapped(x):
+    return jnp.concatenate([x, swap_halves(x)], axis=-1)
+
+
+def project_block(i, rows, heads, nope, vd, lq, lkv, rp, wq, wk, wvt, gq, gk, gq2, gk2, table, q_s, k_s, v_s):
     tok = pl.ds(pl.multiple_of(i * rows, rows), rows)
     wide = wq.shape[1] // heads
     rope2 = wide - nope
@@ -54,19 +48,19 @@
     shared = rp.astype(jnp.float32)
     shared_sq = 0.5 * shared * shared
     lane = lax.broadcasted_iota(jnp.int32, (rows, rope2), 1)
-    tqv, tkv = tq[tok, :], tk[tok, :]
+    tqv, tkv = table[tok, :] * gq2, table[tok, :] * gk2
     for h in range(heads):
         for which in range(2):
             if which == 0:
                 t1 = q[:, h * wide : h * wide + nope]
                 t2 = q[:, h * wide + nope : (h + 1) * wide]
-                sq, gain, table, dest = t1 * t1 + 0.5 * t2 * t2, gq, tqv, q_s
+                sq, gain, turn, dest = t1 * t1 + 0.5 * t2 * t2, gq, tqv, q_s
             else:
                 t1, t2 = k[:, h * nope : (h + 1) * nope], shared
-                sq, gain, table, dest = t1 * t1 + shared_sq, gk, tkv, k_s
+                sq, gain, turn, dest = t1 * t1 + shared_sq, gk, tkv, k_s
             r = lax.rsqrt(jnp.sum(sq, axis=-1, keepdims=True) * inv + EPS)
-            dest[h, tok, 0:nope] = (t1 * r * gain[...]).astype(jnp.bfloat16)
-            y = t2 * r * table
+            dest[h, tok, 0:nope] = (t1 * r * gain).astype(jnp.bfloat16)
+            y = t2 * r * turn
             y = y + pltpu.roll(y, rope2 // 2, 1)
             if which == 1:
                 y = jnp.where(lane < rope2 // 2, y, 0.0)
@@ -146,16 +140,17 @@
 
 
 def sem_count(nx, ny, nz, cores):
-    gather = 4 * ((nx - 1) * cores + cores - 1) + 2 * (nx - 1) * (ny - 1) * cores
+    gather = 5 * ((nx - 1) * cores + cores - 1) + 2 * (nx - 1) * (ny - 1) * cores
     latent = 2 * (2 * (nz - 1) + (2 * nz - 1) * (ny - 1))
-    return gather + latent
+    out = 2 * (nz - 1) + nz * (ny - 1) + nz * ny * (nx - 1) + nz * ny * nx * (cores - 1)
+    return gather + latent + out
 
 
 def layer_kernel(
     dims, chunk, heads, nope, vd, scale,
-    tokens, in_gain, wqd, wld, wrope, q_lat_gain, kv_lat_gain, wqu, wkvu, gq, gk, tq, tk, out_gain,
+    tokens, in_gain, wqd, wld, wrope, q_lat_gain, kv_lat_gain, wqu, wku, wvu, q_gain, k_gain, table, out_gain, w_out,
     out,
-    normed, wqd_g, wld_g, wqu_g, wkvu_g, wvt, kvr_g, q_g, q_s, k_s, v_s, att_s, heads_g,
+    normed, wqd_g, wld_g, wqu_g, wku_g, wvu_g, w_g, wq_s, wvt, kvr_g, q_g, q_s, k_s, v_s, att_s, heads_g,
     send_sems, recv_sems, a2a_send, a2a_recv,
 ):
     nx, ny, nz, cores = dims
@@ -180,7 +175,7 @@
         pl.semaphore_signal(barrier, inc=1, device_id=at_dp(lax.rem(d + k, dps)), device_id_type=MESH)
     pl.semaphore_wait(barrier, seqs + dps - 2)
 
-    weights = ((wqd, wqd_g, True), (wld, wld_g, True), (wqu, wqu_g, False), (wkvu, wkvu_g, False))
+    weights = ((wqd, wqd_g, True), (wld, wld_g, True), (wqu, wqu_g, False), (wku, wku_g, False), (wvu, wvu_g, False))
 
     def piece(ref, split, which):
         part = ref.shape[0] // ny
@@ -193,8 +188,48 @@
             links.send(("x", a, dx), piece(src, split, y), piece(dst.at[d], split, y), at_dp(target))
         for dc, partner in partners:
             links.send(("c", a, dc), src, dst.at[d], at_dp(partner))
+
+    part_out = w_out.shape[0]
+
+    def w_block(zz, yy, xx, cc):
+        first = ((zz * ny + yy) * dps + xx * cores + cc) * part_out
+        return w_g.at[pl.ds(pl.multiple_of(first, part_out), part_out)]
+
+    def w_z(way, step, src, dst, ok):
+        links.send(("wz", way, step), src, dst, at_sp(jnp.clip(z + way, 0, nz - 1) * ny + y), ok)
+
+    def w_z_step(step):
+        for way in (1, -1):
+            origin = z - way * (step + 1)
+            ok = (origin >= 0) & (origin < nz)
+            block = w_block(jnp.clip(origin, 0, nz - 1), y, x, c)
+            links.arrive(("wz", way, step), block, at_sp(s), ok)
+            if step < nz - 2:
+                w_z(way, step + 1, block, block, ok & (z + way >= 0) & (z + way < nz))
+
+    def w_x(k, dy):
+        block = w_block(lax.rem(z + k, nz), lax.rem(y - dy + ny, ny), x, c)
+        for dx in range(1, nx):
+            links.send(("wx", k, dy, dx), block, block, at_dp(lax.rem(x + dx, nx) * cores + c))
+        w_core(k, dy, 0, block)
+
+    def w_core(k, dy, dx, block):
+        for dc, partner in partners:
+            links.send(("wc", k, dy, dx, dc), block, block, at_dp(partner))
+
+    def w_x_arrive(k, dy):
+        for dx in range(1, nx):
+            block = w_block(lax.rem(z + k, nz), lax.rem(y - dy + ny, ny), lax.rem(x - dx + nx, nx), c)
+            links.arrive(("wx", k, dy, dx), block, at_dp(d))
+            w_core(k, dy, dx, block)
+
+    for way in (1, -1):
+        if nz > 1:
+            w_z(way, 0, w_out, w_block(z, y, x, c), (z + way >= 0) & (z + way < nz))
     for src, dst, _ in weights:
         dst[d] = src[...]
+    own_out = pl.ds(pl.multiple_of((s * dps + d) * part_out, part_out), part_out)
+    w_g[own_out, :] = w_out[...]
 
     def norm(i, _):
         step = rows // 4
@@ -214,7 +249,7 @@
             for dc, partner in partners:
                 links.send(("cx", a, dx, dc), got, got, at_dp(partner))
     rope_key = jnp.dot(normed[...], wrope[...], preferred_element_type=jnp.float32)
-    kvr_g[s, :, kr:] = rope_key.astype(jnp.bfloat16)
+    kvr_g[s, :, kr:] = with_swapped(rope_key).astype(jnp.bfloat16)
     for a, (src, dst, split) in enumerate(weights):
         for dx in range(1, nx):
             origin = lax.rem(x - dx + nx, nx) * cores + c
@@ -263,12 +298,18 @@
             if nz > 1:
                 along_z(b, way, 0, s, (z + way >= 0) & (z + way < nz))
 
+    if nz > 1:
+        w_z_step(0)
     settle(1)
     kvr_g[s, :, :kr] = rms_scale(down(wld_g), kv_lat_gain[...]).astype(jnp.bfloat16)
     launch(0)
     settle(0)
     q_g[s] = rms_scale(down(wqd_g), q_lat_gain[...]).astype(jnp.bfloat16)
     launch(1)
+    for step in range(1, nz - 1):
+        w_z_step(step)
+    for k in range(nz):
+        w_x(k, 0)
 
     for step in range(nz - 1):
         for b in range(2):
@@ -280,12 +321,26 @@
                 if step < nz - 2:
                     along_z(b, way, step + 1, slot, ok & (z + way >= 0) & (z + way < nz))
                 over_y(b, way * (step + 1), slot, ok)
+    for k in range(nz):
+        for dy in range(1, ny):
+            block = w_block(lax.rem(z + k, nz), y, x, c)
+            links.send(("wy", k, dy), block, block, at_sp(z * ny + lax.rem(y + dy, ny)))
     settle(2)
     settle(3)
-    wk_cols = heads * nope
-    wq_full = wqu_g.reshape(dps * wqu.shape[0], wqu.shape[1])
-    wkv_full = wkvu_g.reshape(dps * wkvu.shape[0], wkvu.shape[1])
-    wvt[...] = jnp.transpose(wkv_full[:, wk_cols:].astype(jnp.float32)).astype(jnp.bfloat16)
+    settle(4)
+    wk_full = wku_g.reshape(dps * wku.shape[0], wku.shape[1])
+    for k in range(dps):
+        depth = wqu.shape[0]
+        up = wqu_g[k].astype(jnp.float32)
+        columns = []
+        for h in range(heads):
+            head = up[:, h * (wqu.shape[1] // heads) : (h + 1) * (wqu.shape[1] // heads)]
+            columns += [head[:, :nope], with_swapped(head[:, nope:])]
+        wq_s[k * depth : (k + 1) * depth, :] = jnp.concatenate(columns, axis=1).astype(jnp.bfloat16)
+    wv_full = wvu_g.reshape(dps * wvu.shape[0], wvu.shape[1])
+    wvt[...] = jnp.transpose(wv_full[...].astype(jnp.float32)).astype(jnp.bfloat16)
+    gq, gk = q_gain[:, :nope], k_gain[:, :nope]
+    gq2, gk2 = with_swapped(q_gain[:, nope:]), with_swapped(k_gain[:, nope:])
     for b in range(2):
         for tag in range(1 - nz, nz):
             zz = z - tag
@@ -297,7 +352,7 @@
     def project(i, _):
         project_block(
             i, rows, heads, nope, vd, q_g[i], kvr_g[i, :, :kr], kvr_g[i, :, kr:],
-            wq_full, wkv_full.at[:, :wk_cols], wvt, gq, gk, tq, tk, q_s, k_s, v_s,
+            wq_s, wk_full, wvt, gq, gk, gq2, gk2, table, q_s, k_s, v_s,
         )
         return 0
 
@@ -319,7 +374,18 @@
 
         return 0
 
-    lax.fori_loop(0, seqs, attend, 0)
+    lax.fori_loop(0, seqs // 2, attend, 0)
+    for k in range(nz):
+        for dy in range(1, ny):
+            block = w_block(lax.rem(z + k, nz), lax.rem(y - dy + ny, ny), x, c)
+            links.arrive(("wy", k, dy), block, at_sp(s))
+            w_x(k, dy)
+    for k in range(nz):
+        w_x_arrive(k, 0)
+    lax.fori_loop(seqs // 2, seqs, attend, 0)
+    for k in range(nz):
+        for dy in range(1, ny):
+            w_x_arrive(k, dy)
     heads_g[s] = att_s[s]
     for k in range(1, seqs):
         origin = lax.rem(s + k, seqs)
@@ -327,8 +393,6 @@
             src_ref=att_s.at[origin], dst_ref=heads_g.at[origin], send_sem=a2a_send.at[origin],
             recv_sem=a2a_recv.at[origin], device_id=at_sp(origin), device_id_type=MESH,
         ).wait()
-    links.drain()
-
     width = heads * vd
     square = jnp.zeros((rows, 1), jnp.float32)
     for k in range(seqs):
@@ -337,7 +401,25 @@
     r = lax.rsqrt(square * (1.0 / (seqs * width)) + EPS)
     for k in range(seqs):
         cols = slice(k * width, (k + 1) * width)
-        out[:, cols] = (heads_g[k].astype(jnp.float32) * r * out_gain[:, cols]).astype(jnp.bfloat16)
+        normed[:, cols] = (heads_g[k].astype(jnp.float32) * r * out_gain[:, cols]).astype(jnp.bfloat16)
+    for k in range(nz):
+        for dy in range(ny):
+            for dx in range(nx):
+                for dc, _ in partners:
+                    block = w_block(
+                        lax.rem(z + k, nz), lax.rem(y - dy + ny, ny), lax.rem(x - dx + nx, nx),
+                        lax.rem(c - dc + cores, cores),
+                    )
+                    links.arrive(("wc", k, dy, dx, dc), block, at_dp(d))
+    tile = 256 if out.shape[1] % 256 == 0 else out.shape[1]
+
+    def project_out(i, _):
+        cols = pl.ds(pl.multiple_of(i * tile, tile), tile)
+        out[:, cols] = jnp.dot(normed[...], w_g[:, cols], preferred_element_type=jnp.float32).astype(out.dtype)
+        return 0
+
+    lax.fori_loop(0, out.shape[1] // tile, project_out, 0)
+    links.drain()
 
 
 def per_device(
@@ -356,11 +438,6 @@
     nope = w_key_up.shape[1] // heads
     vd = w_value_up.shape[1] // heads
     wide = nope + 2 * rope
-    out_full = lax.all_gather(w_out, ("sp", "dp"), axis=0, tiled=True)
-    tq, tk = tables(length, rope, (query_gain, key_gain))
-    wide_rope = jnp.concatenate([w_rope_key, swap_halves(w_rope_key)], axis=1)
-    wqu = widen_query(w_query_up, heads, rope)
-    wkvu = jnp.concatenate([w_key_up, w_value_up], axis=1)
     chunk = min(2 * own_rows, length)
     sems = sem_count(nx, ny, nz, cores)
     b16 = jnp.bfloat16
@@ -368,16 +445,18 @@
     def gathered(w):
         return pltpu.VMEM((dps,) + w.shape, b16)
 
-    mixed = pl.pallas_call(
+    result = pl.pallas_call(
         functools.partial(
             layer_kernel, (nx, ny, nz, cores), chunk, heads, nope, vd, float(nope + rope) ** -0.5
         ),
-        out_shape=jax.ShapeDtypeStruct((own_rows, seqs * heads * vd), b16),
-        in_specs=[pl.BlockSpec(memory_space=pltpu.VMEM)] * 14,
+        out_shape=jax.ShapeDtypeStruct((own_rows, w_out.shape[1]), b16),
+        in_specs=[pl.BlockSpec(memory_space=pltpu.VMEM)] * 15,
         out_specs=pl.BlockSpec(memory_space=pltpu.VMEM),
         scratch_shapes=[
-            pltpu.VMEM((own_rows, tokens.shape[2]), b16),
-            gathered(w_query_down), gathered(w_latent_down), gathered(wqu), gathered(wkvu),
+            pltpu.VMEM((own_rows, max(tokens.shape[2], w_out.shape[0] * seqs * dps)), b16),
+            gathered(w_query_down), gathered(w_latent_down), gathered(w_query_up), gathered(w_key_up), gathered(w_value_up),
+            pltpu.VMEM((w_out.shape[0] * seqs * dps, w_out.shape[1]), b16),
+            pltpu.VMEM((w_query_down.shape[1], heads * wide), b16),
             pltpu.VMEM((heads * vd, w_latent_down.shape[1]), b16),
             pltpu.VMEM((seqs, own_rows, w_latent_down.shape[1] + 2 * rope), b16),
             pltpu.VMEM((seqs, own_rows, w_query_down.shape[1]), b16),
@@ -396,12 +475,11 @@
         ),
         cost_estimate=pl.CostEstimate(flops=60 * 10**9, bytes_accessed=10**8, transcendentals=5 * 10**6),
     )(
-        tokens.reshape(own_rows, tokens.shape[2]), in_gain[None], w_query_down, w_latent_down, wide_rope,
-        query_latent_gain[None], latent_gain[None], wqu, wkvu,
-        query_gain[None, :nope], key_gain[None, :nope], tq, tk, out_gain[None],
+        tokens.reshape(own_rows, tokens.shape[2]), in_gain[None], w_query_down, w_latent_down, w_rope_key,
+        query_latent_gain[None], latent_gain[None], w_query_up, w_key_up, w_value_up,
+        query_gain[None], key_gain[None], jnp.asarray(rotation_table(length, rope)), out_gain[None], w_out,
     )
-    projected = jnp.dot(mixed, out_full, preferred_element_type=jnp.float32)
-    return projected.astype(b16).reshape(1, own_rows, w_out.shape[1])
+    return result.reshape(1, own_rows, w_out.shape[1])
 
 
 def solution(mesh):

time: 165 us -> 132 us (0.80)
  between operations: 13.4 us -> 0.01 us
  other arithmetic: 8.88 us -> 0 us
  matrix products: 7.02 us -> 0 us
  local copies, waits for them, and re-layouts: 7.52 us -> 4.26 us
    dot_general x1 -> x0, matrix products: 7.02 us -> none  [per_device(): projected = jnp.dot(mixed, out_full, preferred_element_type=jnp.float32)]
    cos x1 -> x0, other arithmetic: 3.89 us -> none  [tables(): cosine, sine = (jnp.cos(angles), jnp.sin(angles))]
    slice x6 -> x0, local copies, waits for them, and re-layouts: 3.23 us -> none  [the longest x4 1.87 us: swap_halves(): return jnp.concatenate([x[..., half:], x[..., :half]], axis=-1)]
    concatenate x4 -> x0, other arithmetic: 2.8 us -> none  [the longest x1 1.41 us: per_device(): wkvu = jnp.concatenate([w_key_up, w_value_up], axis=1)]
    mul x1 -> x0, other arithmetic: 2.18 us -> none  [tables(): out.append(base * jnp.concatenate([tail, swap_halves(tail)])[None, :])]
    unnamed x2, local copies, waits for them, and re-layouts: 2.23 us -> 4.26 us
  transfers between devices with their start and end apart: 1 -> 0, of which waited for: 0 -> 0; matrix products, arithmetic and copies ran while one was open for 10% -> 0% of each run, Pallas kernels for 77% -> 0%
where the time goes in v3:
time: 132 us
  Pallas kernels  128 us (97%)
  local copies, waits for them, and re-layouts  4.26 us (3%)
    pallas_call x1, Pallas kernels, per_device(): pl.pallas_call(functools.partial(layer_kernel, (nx, ny, nz, cores), chunk...  128 us
    unnamed x2, local copies, waits for them, and re-layouts  4.26 us

profile of v3, /device:TPU:0, one launch (start us, length us, event | category | flops | bytes accessed | tf_op | source)
XLA Modules:
  0.0 132.0 jit_solution(1645479321639968264)
XLA Ops:
  0.0 2.0 %copy.16.wrope = bf16[2048,64]{1,0:T(8,128)(2,1)} copy(bf16[2048,64]{0,1:T(8,128)(2,1)} %param.19) | data formatting | bytes 524288 | tf_op args[4]
  2.0 127.8 %shard_map.145 = bf16[256,2048]{1,0:T(8,128)(2,1)} custom-call(bf16[256,2048]{1,0:T(8,128)(2,1)} %bitcast.9, f32[1,2048]{1,0:T(1,128)} %bitcast.10, bf16[512,512]{1,0:T(8,128)(2,1)} %wqd.1, bf16[512,256]{1,0:T(8,128)(2,1)} %wld.1, bf16[2048,64]{1,0:T(8,128)(2,1)} %copy.16.wrope, f32[1,512]{1,0:T(1,128)} %bitcast.12, f32[1,256]{1,0:T(1,128)} %bitcast.13, ...), custom_call_target="tpu_custom_call" | custom-call | flops 60000002048 | bytes 100000000 | tf_op jit(solution)/shard_map/pallas_call | solution.py:448
  129.7 2.3 %copy.18 = bf16[1,256,2048]{2,1,0:T(8,128)(2,1)} copy(bf16[1,256,2048]{2,1,0:T(8,128)(2,1)} %bitcast.8) | data formatting | bytes 2097152

commit v4 on v3

--- a/solution.py
+++ b/solution.py
@@ -175,7 +175,7 @@
         pl.semaphore_signal(barrier, inc=1, device_id=at_dp(lax.rem(d + k, dps)), device_id_type=MESH)
     pl.semaphore_wait(barrier, seqs + dps - 2)
 
-    weights = ((wqd, wqd_g, True), (wld, wld_g, True), (wqu, wqu_g, False), (wku, wku_g, False), (wvu, wvu_g, False))
+    weights = ((wld, wld_g, True), (wqd, wqd_g, True), (wqu, wqu_g, False), (wku, wku_g, False), (wvu, wvu_g, False))
 
     def piece(ref, split, which):
         part = ref.shape[0] // ny
@@ -239,7 +239,8 @@
 
     lax.fori_loop(0, 4, norm, 0)
 
-    for a, (src, dst, split) in enumerate(weights):
+    def relay(a):
+        src, dst, split = weights[a]
         for dx in range(1, nx):
             origin = lax.rem(x - dx + nx, nx) * cores + c
             got = piece(dst.at[origin], split, y)
@@ -248,9 +249,6 @@
                 links.send(("y", a, dx, dy), got, got, at_sp(z * ny + lax.rem(y + dy, ny)))
             for dc, partner in partners:
                 links.send(("cx", a, dx, dc), got, got, at_dp(partner))
-    rope_key = jnp.dot(normed[...], wrope[...], preferred_element_type=jnp.float32)
-    kvr_g[s, :, kr:] = with_swapped(rope_key).astype(jnp.bfloat16)
-    for a, (src, dst, split) in enumerate(weights):
         for dx in range(1, nx):
             origin = lax.rem(x - dx + nx, nx) * cores + c
             for dy in range(1, ny if split else 1):
@@ -258,6 +256,9 @@
                 links.arrive(("y", a, dx, dy), got, at_dp(d))
                 for dc, partner in partners:
                     links.send(("cy", a, dx, dy, dc), got, got, at_dp(partner))
+
+    rope_key = jnp.dot(normed[:, : tokens.shape[1]], wrope[...], preferred_element_type=jnp.float32)
+    kvr_g[s, :, kr:] = with_swapped(rope_key).astype(jnp.bfloat16)
 
     def settle(a):
         src, dst, split = weights[a]
@@ -298,14 +299,18 @@
             if nz > 1:
                 along_z(b, way, 0, s, (z + way >= 0) & (z + way < nz))
 
+    relay(0)
+    settle(0)
+    kvr_g[s, :, :kr] = rms_scale(down(wld_g), kv_lat_gain[...]).astype(jnp.bfloat16)
+    launch(0)
+    relay(1)
+    settle(1)
+    q_g[s] = rms_scale(down(wqd_g), q_lat_gain[...]).astype(jnp.bfloat16)
+    launch(1)
     if nz > 1:
         w_z_step(0)
-    settle(1)
-    kvr_g[s, :, :kr] = rms_scale(down(wld_g), kv_lat_gain[...]).astype(jnp.bfloat16)
-    launch(0)
-    settle(0)
-    q_g[s] = rms_scale(down(wqd_g), q_lat_gain[...]).astype(jnp.bfloat16)
-    launch(1)
+    for a in range(2, len(weights)):
+        relay(a)
     for step in range(1, nz - 1):
         w_z_step(step)
     for k in range(nz):
@@ -341,6 +346,15 @@
     wvt[...] = jnp.transpose(wv_full[...].astype(jnp.float32)).astype(jnp.bfloat16)
     gq, gk = q_gain[:, :nope], k_gain[:, :nope]
     gq2, gk2 = with_swapped(q_gain[:, nope:]), with_swapped(k_gain[:, nope:])
+    def project(j, _):
+        i = lax.rem(j, nz) * ny + lax.rem(y + lax.div(j, nz), ny)
+        project_block(
+            i, rows, heads, nope, vd, q_g[i], kvr_g[i, :, :kr], kvr_g[i, :, kr:],
+            wq_s, wk_full, wvt, gq, gk, gq2, gk2, table, q_s, k_s, v_s,
+        )
+        return 0
+
+    lax.fori_loop(0, nz, project, 0)
     for b in range(2):
         for tag in range(1 - nz, nz):
             zz = z - tag
@@ -348,15 +362,7 @@
             for dy in range(1, ny):
                 slot = jnp.clip(zz, 0, nz - 1) * ny + lax.rem(y - dy + ny, ny)
                 links.arrive(("ly", b, tag, dy), buffers[b].at[slot], at_sp(s), ok)
-
-    def project(i, _):
-        project_block(
-            i, rows, heads, nope, vd, q_g[i], kvr_g[i, :, :kr], kvr_g[i, :, kr:],
-            wq_s, wk_full, wvt, gq, gk, gq2, gk2, table, q_s, k_s, v_s,
-        )
-        return 0
-
-    lax.fori_loop(0, seqs, project, 0)
+    lax.fori_loop(nz, seqs, project, 0)
 
     def hand_over(qb):
         return pltpu.make_async_remote_copy(

time: 132 us -> 139 us (1.053)
  Pallas kernels: 128 us -> 135 us
    pallas_call x1, Pallas kernels: 128 us -> 135 us  [per_device(): pl.pallas_call(functools.partial(layer_kernel, (nx, ny, nz, cores), chunk...]
where the time goes in v4:
time: 139 us
  Pallas kernels  135 us (97%)
  local copies, waits for them, and re-layouts  4.26 us (3%)
    pallas_call x1, Pallas kernels, per_device(): pl.pallas_call(functools.partial(layer_kernel, (nx, ny, nz, cores), chunk...  135 us
    unnamed x2, local copies, waits for them, and re-layouts  4.26 us

profile of v4, /device:TPU:0, one launch (start us, length us, event | category | flops | bytes accessed | tf_op | source)
XLA Modules:
  0.0 138.8 jit_solution(13293674004926435386)
XLA Ops:
  0.0 2.0 %copy.16.wrope = bf16[2048,64]{1,0:T(8,128)(2,1)} copy(bf16[2048,64]{0,1:T(8,128)(2,1)} %param.19) | data formatting | bytes 524288 | tf_op args[4]
  2.0 134.5 %shard_map.145 = bf16[256,2048]{1,0:T(8,128)(2,1)} custom-call(bf16[256,2048]{1,0:T(8,128)(2,1)} %bitcast.9, f32[1,2048]{1,0:T(1,128)} %bitcast.10, bf16[512,512]{1,0:T(8,128)(2,1)} %wqd.1, bf16[512,256]{1,0:T(8,128)(2,1)} %wld.1, bf16[2048,64]{1,0:T(8,128)(2,1)} %copy.16.wrope, f32[1,512]{1,0:T(1,128)} %bitcast.12, f32[1,256]{1,0:T(1,128)} %bitcast.13, ...), custom_call_target="tpu_custom_call" | custom-call | flops 60000002048 | bytes 100000000 | tf_op jit(solution)/shard_map/pallas_call | solution.py:454
  136.5 2.3 %copy.18 = bf16[1,256,2048]{2,1,0:T(8,128)(2,1)} copy(bf16[1,256,2048]{2,1,0:T(8,128)(2,1)} %bitcast.8) | data formatting | bytes 2097152
